TPU v7x, 128 devices: a whole 4x4x4 slice. The times are simulated.
128 devices in a mesh: sp: 16 (over z, y), dp: 8 (over x, core).
Axes of the slice: x: 4, y: 4, z: 4, core: 2. Of those that a mesh axis runs over, the one named last changes fastest.
Arguments:
- stream: bfloat16 [8, 2048, 2048], P('dp', 'sp'), may hold values from -6 to 6
- query_proj: bfloat16 [8, 2048, 2048], P('dp', 'sp'), may hold values from -6 to 6
- key_proj: bfloat16 [8, 2048, 2048], P('dp', 'sp'), may hold values from -6 to 6
- value_proj: bfloat16 [8, 2048, 2048], P('dp', 'sp'), may hold values from -6 to 6
- out_gate: bfloat16 [8, 2048, 2048], P('dp', 'sp'), may hold values from -6 to 6
- beta_logit: bfloat16 [8, 2048, 16], P('dp', 'sp'), may hold values from -6 to 6
- log_decay: float32 [8, 16, 2048], P('dp', 'sp'), may hold values from -0.8 to 0, as said below
- head_gain: float32 [128], replicated, may hold values from 0.1 to 1.9
- out_proj: bfloat16 [2048, 2048], replicated, may hold values from -0.125 to 0.125
- ffn_gain: float32 [2048], replicated, may hold values from 0.1 to 1.9
- routes: int32 [8, 2048, 2], P('dp', 'sp'), may hold values from 0 to 15, all different within a row; in each aligned block of 128 rows (0 to 127, 128 to 255, ..., all dimensions but the last counted through in order) at most 32 rows name the same one
- route_weight: float32 [8, 2048, 2], P('dp', 'sp'), may hold values from 0.1 to 1
- expert_gate: bfloat16 [16, 2048, 5120], P('sp', None, 'dp'), may hold values from -0.125 to 0.125
- expert_up: bfloat16 [16, 2048, 5120], P('sp', None, 'dp'), may hold values from -0.125 to 0.125
- expert_down: bfloat16 [16, 5120, 2048], P('sp', 'dp'), may hold values from -0.078125 to 0.078125
Outputs:
- result: bfloat16 [8, 2048, 2048], P('dp', 'sp')
Inputs may be any that keep to these rules, and one draw needn't show every extreme that they name: `routes`: each row names 2 different experts; within the rows of one device no expert is named more than 32 times, and some devices reach 32. log_decay is never positive.
All inputs are finite; a program needn't handle non-finite values.
Results may differ from a plain program's by a relative error of at most 0.0085.
Values may be sent and summed in bfloat16 or wider, within the bound.
No kernel may reach another device: no remote copies, remote signals or barrier semaphores. Data moves between devices by JAX's collectives and lax.ppermute only.
A program may use at most 128 MiB of HBM per device.

v0:
```python
import jax
import jax.numpy as jnp
from jax import lax
from jax.experimental import pallas as pl
from jax.experimental.pallas import tpu as pltpu
from jax.sharding import PartitionSpec as P

EPSILON = 1e-6
HEAD_DIM = 128
TOK = 128
BASE = 16
UNROLL = 2


def mm(a, b):
    return jnp.dot(a, b, preferred_element_type=jnp.float32)


def halves(a):
    high = a.astype(jnp.bfloat16)
    return high, (a - high.astype(jnp.float32)).astype(jnp.bfloat16)


def mm3(a, b):
    ah, al = halves(a)
    bh, bl = halves(b)
    return mm(ah, bh) + (mm(ah, bl) + mm(al, bh))


def unit_lower_inverse(low, rows, cols):
    n = low.shape[0]
    group = cols[:BASE] // BASE
    packed = jnp.where(group == 0, low[:BASE], 0.0)
    for b in range(1, n // BASE):
        packed = packed + jnp.where(group == b, low[b * BASE : (b + 1) * BASE], 0.0)
    inv = jnp.where(rows[:BASE] == cols[:BASE] % BASE, 1.0, 0.0)
    for j in range(BASE - 1):
        column = jnp.take_along_axis(packed, group * BASE + j, axis=1)
        inv = inv - column * inv[j : j + 1]
    full = jnp.concatenate([jnp.where(group == b, inv, 0.0) for b in range(n // BASE)], axis=0)
    width = BASE
    while width < n:
        off = (rows // (2 * width) == cols // (2 * width)) & (rows // width != cols // width)
        full = full - mm3(full, mm3(jnp.where(off, low, 0.0), full))
        width *= 2
    return full


def mixer_kernel(recv_ref, rate_ref, out_ref, vec_ref, step_ref, add_ref, acc_ref):
    n_blk = recv_ref.shape[0]
    rows = lax.broadcasted_iota(jnp.int32, (TOK, TOK), 0)
    cols = lax.broadcasted_iota(jnp.int32, (TOK, TOK), 1)
    rate = rate_ref[...]
    before = jnp.where(rows <= cols, 1.0, 0.0)
    after = jnp.where(rows >= cols, 1.0, 0.0)
    fwd_sum = jnp.dot(rate, before, precision=lax.Precision.HIGHEST, preferred_element_type=jnp.float32)
    bwd_sum = jnp.dot(rate, after, precision=lax.Precision.HIGHEST, preferred_element_type=jnp.float32)
    for n in range(n_blk):
        logit = recv_ref[n, 3 * TOK : 3 * TOK + 16, :].astype(jnp.float32)[0:1]
        vec_ref[n, 0:1, :] = fwd_sum[n : n + 1]
        vec_ref[n, 1:2, :] = bwd_sum[n : n + 1]
        vec_ref[n, 2:3, :] = jax.nn.sigmoid(logit)
        vec_ref[n, 3:4, :] = jnp.broadcast_to(fwd_sum[n : n + 1, TOK - 1 : TOK], (1, TOK))
        vec_ref[n, 4:8, :] = jnp.zeros((4, TOK), jnp.float32)

    def prepare(n):
        query = recv_ref[n, 0:TOK, :]
        key = recv_ref[n, TOK : 2 * TOK, :]
        query_f = query.astype(jnp.float32)
        key_f = key.astype(jnp.float32)
        value_f = recv_ref[n, 2 * TOK : 3 * TOK, :].astype(jnp.float32)
        key_tf = key_f.T
        key_t = key_tf.astype(jnp.bfloat16)
        key_c = lax.rsqrt(jnp.sum(key_f * key_f, axis=1, keepdims=True) + EPSILON)
        key_r = lax.rsqrt(jnp.sum(key_tf * key_tf, axis=0, keepdims=True) + EPSILON)
        query_c = lax.rsqrt(jnp.sum(query_f * query_f, axis=1, keepdims=True) + EPSILON) * HEAD_DIM ** (-0.5)
        vec_r = vec_ref[n]
        vec_c = vec_r.T
        beta_r, beta_c = vec_r[2:3], vec_c[:, 2:3]
        total = vec_r[3:4]
        kk = mm(key, key_t) * key_c * key_r
        qk = mm(query, key_t) * query_c * key_r
        acc = None
        for d in range(2):
            sum_r, sum_c = vec_r[d : d + 1], vec_c[:, d : d + 1]
            gap = sum_c - sum_r
            if d == 0:
                decay = jnp.exp(jnp.where(rows >= cols, gap, -jnp.inf))
                low = jnp.where(rows > cols, kk * decay, 0.0) * beta_c
                solve = unit_lower_inverse(low, rows, cols)
            else:
                decay = jnp.exp(jnp.where(rows <= cols, gap, -jnp.inf))
                low = jnp.where(rows > cols, kk * jnp.exp(jnp.where(rows >= cols, -gap, -jnp.inf)), 0.0) * beta_r
                solve = unit_lower_inverse(low, rows, cols).T
            grown = jnp.exp(sum_c)
            rhs = jnp.concatenate([value_f * beta_c, key_f * (beta_c * key_c * grown)], axis=1)
            both = mm(solve.astype(jnp.bfloat16), rhs.astype(jnp.bfloat16)).astype(jnp.bfloat16)
            lhs = jnp.concatenate([qk * decay, key_tf * (key_r * jnp.exp(total - sum_r))], axis=0)
            done = mm(lhs.astype(jnp.bfloat16), both)
            step_ref[d, n, 0:TOK, :] = (query_f * (query_c * grown) - done[:TOK, HEAD_DIM:]).astype(jnp.bfloat16)
            step_ref[d, n, TOK:, :] = done[TOK:, HEAD_DIM:].astype(jnp.bfloat16)
            add_ref[d, n] = done[TOK:, :HEAD_DIM]
            acc = done[:TOK, :HEAD_DIM] if acc is None else acc + done[:TOK, :HEAD_DIM]
        acc_ref[n] = acc

    def prepare_group(i, carry):
        for u in range(UNROLL):
            prepare(i * UNROLL + u)
        return carry

    lax.fori_loop(0, n_blk // UNROLL, prepare_group, 0)

    def walk(t, states):
        after_step = []
        for d, state in enumerate(states):
            n = t if d == 0 else n_blk - 1 - t
            high, low = halves(state)
            got = mm(step_ref[d, n], jnp.concatenate([high, low], axis=1))
            got = got[:, :HEAD_DIM] + got[:, HEAD_DIM:]
            acc_ref[n] = acc_ref[n] + got[:TOK]
            keep = jnp.exp(vec_ref[n][3:4])
            after_step.append(state * keep - got[TOK:] + add_ref[d, n])
        return tuple(after_step)

    zero = jnp.zeros((HEAD_DIM, HEAD_DIM), jnp.float32)
    lax.fori_loop(0, n_blk, walk, (zero, zero))
    out_ref[...] = acc_ref[...].astype(jnp.bfloat16)


def mixer(recv, rate, interpret=False):
    n_blk = recv.shape[0]
    return pl.pallas_call(
        mixer_kernel,
        out_shape=jax.ShapeDtypeStruct((n_blk, TOK, HEAD_DIM), jnp.bfloat16),
        in_specs=[pl.BlockSpec(memory_space=pltpu.VMEM)] * 2,
        out_specs=pl.BlockSpec(memory_space=pltpu.VMEM),
        scratch_shapes=[
            pltpu.VMEM((n_blk, 8, TOK), jnp.float32),
            pltpu.VMEM((2, n_blk, 2 * TOK, HEAD_DIM), jnp.bfloat16),
            pltpu.VMEM((2, n_blk, HEAD_DIM, HEAD_DIM), jnp.float32),
            pltpu.VMEM((n_blk, TOK, HEAD_DIM), jnp.float32),
        ],
        name="mixer",
        interpret=interpret,
    )(recv, rate)


def expert_part(rows, gate_local, up_local, down_local):
    gate_act = jnp.dot(rows, gate_local, preferred_element_type=jnp.float32)
    up_act = jnp.dot(rows, up_local, preferred_element_type=jnp.float32)
    hidden = (jax.nn.silu(gate_act) * up_act).astype(jnp.bfloat16)
    return jnp.dot(hidden, down_local, preferred_element_type=jnp.float32)


def body(
    stream,
    query_proj,
    key_proj,
    value_proj,
    out_gate,
    beta_logit,
    log_decay,
    head_gain,
    out_proj,
    ffn_gain,
    routes,
    route_weight,
    expert_gate,
    expert_up,
    expert_down,
):
    tok_count = stream.shape[1]
    model_width = stream.shape[2]
    n_heads = beta_logit.shape[2]

    def by_head(tensor):
        return tensor[0].reshape(tok_count, n_heads, HEAD_DIM).transpose(1, 0, 2)

    logits = jnp.pad(beta_logit[0].T[:, None, :], ((0, 0), (0, 15), (0, 0)))
    payload = jnp.concatenate(
        [by_head(query_proj), by_head(key_proj), by_head(value_proj), logits], axis=1
    )
    received = lax.all_to_all(payload, "sp", split_axis=0, concat_axis=0, tiled=True)
    mixed = mixer(received, log_decay.reshape(-1, TOK))
    tokens_view = lax.all_to_all(mixed, "sp", split_axis=0, concat_axis=0, tiled=True)
    per_head = tokens_view.astype(jnp.float32)
    normed_heads = (
        per_head
        * lax.rsqrt(jnp.mean(per_head * per_head, axis=-1, keepdims=True) + EPSILON)
        * head_gain
    )
    gated = (
        normed_heads.transpose(1, 0, 2).reshape(tok_count, -1) * jax.nn.silu(out_gate[0].astype(jnp.float32))
    ).astype(jnp.bfloat16)
    resid = stream[0].astype(jnp.float32) + jnp.dot(
        gated, out_proj, preferred_element_type=jnp.float32
    )
    ffn_in = (
        resid * lax.rsqrt(jnp.mean(resid * resid, axis=-1, keepdims=True) + EPSILON) * ffn_gain
    ).astype(jnp.bfloat16)
    n_sp = lax.axis_size("sp")
    top_count = routes.shape[2]
    capacity = tok_count * top_count * 2 // n_sp
    flat_routes = routes.reshape(-1)
    expert_ids = lax.broadcasted_iota(jnp.int32, (1, n_sp), 1)
    chosen = (flat_routes[:, None] == expert_ids).astype(jnp.int32)
    earlier = jnp.cumsum(chosen, axis=0) - chosen
    slot_ids = flat_routes * capacity + jnp.sum(earlier * chosen, axis=1)
    slot_grid = lax.broadcasted_iota(jnp.int32, (n_sp * capacity, 1), 0)
    placing = (
        (slot_grid == slot_ids[None, :])
        .astype(jnp.int32)
        .reshape(n_sp * capacity, tok_count, top_count)
    )
    placing = jnp.sum(placing, axis=2).astype(jnp.bfloat16)
    outgoing = jnp.dot(placing, ffn_in, preferred_element_type=jnp.float32).astype(jnp.bfloat16)
    outgoing = outgoing.reshape(n_sp, capacity, model_width)
    gate_local = expert_gate[0]
    up_local = expert_up[0]
    down_local = expert_down[0]
    arrived = lax.all_to_all(outgoing, "sp", split_axis=0, concat_axis=0, tiled=True)
    piece = lax.all_gather(arrived, "dp", axis=0, tiled=True)
    flat_rows = piece.reshape(-1, model_width)
    partial_value = expert_part(flat_rows, gate_local, up_local, down_local).reshape(
        piece.shape[0], piece.shape[1], model_width
    )
    summed = lax.psum_scatter(
        partial_value.astype(jnp.bfloat16), "dp", scatter_dimension=0, tiled=True
    )
    returned = lax.all_to_all(summed, "sp", split_axis=0, concat_axis=0, tiled=True)
    picked = returned.reshape(n_sp * capacity, model_width)[slot_ids]
    picked = picked.reshape(tok_count, top_count, model_width).astype(jnp.float32)
    routed = jnp.sum(picked * route_weight[0][..., None], axis=1)
    return (resid + routed).astype(jnp.bfloat16)[None]


def solution(mesh):
    return jax.shard_map(
        body,
        mesh=mesh,
        in_specs=(
            P("dp", "sp", None),
            P("dp", "sp", None),
            P("dp", "sp", None),
            P("dp", "sp", None),
            P("dp", "sp", None),
            P("dp", "sp", None),
            P("dp", "sp", None),
            P(),
            P(),
            P(),
            P("dp", "sp", None),
            P("dp", "sp", None),
            P("sp", None, "dp"),
            P("sp", None, "dp"),
            P("sp", "dp", None),
        ),
        out_specs=P("dp", "sp", None),
        check_vma=False,
    )
```

profile of v0, /device:TPU:3, one launch (start us, length us, event | category | flops | bytes accessed | tf_op | source)
XLA Modules:
  0.0 456.1 jit_solution(10732082489127109695)
XLA Ops:
  6.5 2.2 copy.51
  10.1 2.0 copy.53
  12.1 2.0 copy.54
  18.2 2.5 fusion.6
  20.8 7.8 %all-to-all-start = ((bf16[16,400,128]{2,1,0:T(8,128)(2,1)}), bf16[16,400,128]{2,1,0:T(8,128)(2,1)}, u32[]{:S(2)}, u32[]{:S(2)}) async-start(bf16[16,400,128]{2,1,0:T(8,128)(2,1)} %fusion.6), calls=%async_computation | async-start | bytes 3276800 | tf_op jit(solution)/shard_map/all_to_all | solution.py:183
  29.5 23.2 %all-to-all-done.recv_ref = bf16[16,400,128]{2,1,0:T(8,128)(2,1)} async-done(((bf16[16,400,128]{2,1,0:T(8,128)(2,1)}), bf16[16,400,128]{2,1,0:T(8,128)(2,1)}, u32[]{:S(2)}, u32[]{:S(2)}) %all-to-all-start) | async-done | bytes 1638432 | tf_op jit(solution)/shard_map/all_to_all | solution.py:183
  52.6 48.4 %mixer.1 = bf16[16,128,128]{2,1,0:T(8,128)(2,1)} custom-call(bf16[16,400,128]{2,1,0:T(8,128)(2,1)} %all-to-all-done.recv_ref, f32[16,128]{1,0:T(8,128)} %bitcast.76), custom_call_target="tpu_custom_call" | custom-call | tf_op jit(solution)/shard_map/mixer/pallas_call | solution.py:132
  101.0 4.5 all-to-all-start.1
  106.2 2.1 copy.59
  108.4 7.4 %all-to-all-done.1 = bf16[16,128,128]{2,1,0:T(8,128)(2,1)S(1)} async-done(((bf16[16,128,128]{2,1,0:T(8,128)(2,1)}), bf16[16,128,128]{2,1,0:T(8,128)(2,1)S(1)}, u32[]{:S(2)}, u32[]{:S(2)}) %all-to-all-start.1) | async-done | bytes 524320 | tf_op jit(solution)/shard_map/all_to_all | solution.py:185
  117.6 2.6 copy.58
  121.8 4.8 %multiply_reduce_fusion.1 = (f32[128]{0:T(128)S(1)}, f32[128,2048]{1,0:T(8,128)S(1)}) fusion(bf16[128,2048]{0,1:T(8,128)(2,1)S(1)} %fusion.14, bf16[2048,2048]{1,0:T(8,128)(2,1)} %param.23, bf16[1,128,2048]{2,1,0:T(8,128)(2,1)S(1)} %copy-done.3), kind=kOutput, calls=%fused_computation.27 | convolution fusion | flops 1074790272 | bytes 10486272 | tf_op jit(solution)/shard_map/dot_general | solution.py:195
  128.4 30.6 %all_to_all.20 = bf16[16,32,2048]{2,1,0:T(8,128)(2,1)} all-to-all(bf16[16,32,2048]{2,1,0:T(8,128)(2,1)S(1)} %bitcast.68), channel_id=1, replica_groups=mesh['sp'=16,'dp'=8] {'sp'}, dimensions={0} | all-to-all | bytes 4194304 | tf_op jit(solution)/shard_map/all_to_all | solution.py:221
  159.2 84.0 %all-gather.2.cloned.1.call-done = bf16[128,32,2048]{2,1,0:T(8,128)(2,1)} async-done(((bf16[16,32,2048]{2,1,0:T(8,128)(2,1)}), bf16[128,32,2048]{2,1,0:T(8,128)(2,1)}) %all-gather.2.cloned.1.call-update) | async-done | bytes 16777232 | tf_op jit(solution)/shard_map/all_gather | solution.py:222
  243.2 19.1 %fusion.4 = f32[4096,640]{1,0:T(8,128)} fusion(bf16[4096,2048]{1,0:T(8,128)(2,1)} %bitcast.80, bf16[1,2048,640]{2,1,0:T(8,128)(2,1)} %param.27), kind=kOutput, calls=%fused_computation.9 | convolution fusion | flops 10737418240 | bytes 29884416 | tf_op jit(solution)/shard_map/dot_general | solution.py:149
  262.3 19.5 %multiply_convert_fusion = bf16[4096,640]{1,0:T(8,128)(2,1)S(1)} fusion(f32[4096,640]{1,0:T(8,128)} %fusion.4, bf16[4096,2048]{1,0:T(8,128)(2,1)} %bitcast.81, bf16[1,2048,640]{2,1,0:T(8,128)(2,1)S(1)} %copy-done.9), kind=kOutput, calls=%fused_computation.2 | convolution fusion | flops 10753146880 | bytes 35127296 | tf_op jit(solution)/shard_map/dot_general | solution.py:150
  281.7 16.0 %convolution_convert_fusion = bf16[128,32,2048]{2,0,1:T(8,128)(2,1)} fusion(bf16[128,32,640]{2,1,0:T(8,128)(2,1)S(1)} %bitcast.82, bf16[1,640,2048]{2,1,0:T(8,128)(2,1)S(1)} %copy-done), kind=kOutput, calls=%fused_computation.1 | convolution fusion | flops 10745806848 | bytes 24641536 | tf_op jit(solution)/shard_map/dot_general | solution.py:152
  297.8 91.6 %reduce-scatter.2.cloned.1.call-done = bf16[16,32,2048]{2,0,1:T(8,128)(2,1)} async-done(((bf16[128,32,2048]{2,0,1:T(8,128)(2,1)}), bf16[16,32,2048]{2,0,1:T(8,128)(2,1)}) %reduce-scatter.2.cloned.1.call-update) | async-done | bytes 2097168 | tf_op jit(solution)/shard_map/reduce_scatter | solution.py:227
  389.4 4.0 copy.66
  393.4 6.7 %all-to-all-start.3 = ((bf16[16,32,2048]{2,1,0:T(8,128)(2,1)}), bf16[16,32,2048]{2,1,0:T(8,128)(2,1)}, u32[]{:S(2)}, u32[]{:S(2)}) async-start(bf16[16,32,2048]{2,1,0:T(8,128)(2,1)} %copy.66), calls=%async_computation.4 | async-start | bytes 4194304 | tf_op jit(solution)/shard_map/all_to_all | solution.py:230
  400.5 34.3 %all-to-all-done.3 = bf16[16,32,2048]{2,1,0:T(8,128)(2,1)} async-done(((bf16[16,32,2048]{2,1,0:T(8,128)(2,1)}), bf16[16,32,2048]{2,1,0:T(8,128)(2,1)}, u32[]{:S(2)}, u32[]{:S(2)}) %all-to-all-start.3) | async-done | bytes 2097184 | tf_op jit(solution)/shard_map/all_to_all | solution.py:230
  434.8 5.2 %gather_fusion = bf16[256,2048]{1,0:T(8,128)(2,1)} fusion(bf16[512,2048]{1,0:T(8,128)(2,1)} %bitcast.24, s32[1024]{0:T(1024)S(1)} %pad_clamp_fusion), kind=kCustom, calls=%fused_computation | custom fusion | bytes 2098176 | tf_op jit(solution)/shard_map/gather | solution.py:231
  440.0 3.4 reshape.117
  443.4 4.9 %multiply_reduce_fusion = f32[128,2048]{1,0:T(8,128)S(1)} fusion(f32[128,2,2048]{2,1,0:T(2,128)} %reshape.117, f32[128,2]{1,0:T(8,128)S(1)} %copy.67), kind=kLoop, calls=%fused_computation.12 | loop fusion | flops 786432 | bytes 3146752 | tf_op jit(solution)/shard_map/reduce_sum | solution.py:233
  (53 shorter events, 13.6 us)
Async XLA Ops:
  6.5 275.2 %copy-start = (bf16[1,640,2048]{2,1,0:T(8,128)(2,1)S(1)}, bf16[1,640,2048]{2,1,0:T(8,128)(2,1)}, u32[]{:S(2)}) copy-start(bf16[1,640,2048]{2,1,0:T(8,128)(2,1)} %param.29) | copy-start | bytes 7864324
  6.5 11.7 %copy-start.5 = (bf16[1,128,16]{1,2,0:T(8,128)(2,1)S(1)}, bf16[1,128,16]{1,2,0:T(8,128)(2,1)}, u32[]{:S(2)}) copy-start(bf16[1,128,16]{1,2,0:T(8,128)(2,1)} %param.20) | copy-start | bytes 12292
  18.2 10.4 %copy-start.6 = (s32[1,128,2]{1,2,0:T(2,128)S(1)}, s32[1,128,2]{1,2,0:T(2,128)}, u32[]{:S(2)}) copy-start(s32[1,128,2]{1,2,0:T(2,128)} %param.25) | copy-start | bytes 3076
  20.8 31.9 %all-to-all-start = ((bf16[16,400,128]{2,1,0:T(8,128)(2,1)}), bf16[16,400,128]{2,1,0:T(8,128)(2,1)}, u32[]{:S(2)}, u32[]{:S(2)}) async-start(bf16[16,400,128]{2,1,0:T(8,128)(2,1)} %fusion.6), calls=%async_computation | async-start | bytes 3276800 | tf_op jit(solution)/shard_map/all_to_all | solution.py:183
  28.6 87.6 %copy-start.8 = (f32[128]{0:T(128)S(1)}, f32[128]{0:T(128)}, u32[]{:S(2)}) copy-start(f32[128]{0:T(128)} %param.22) | copy-start | bytes 1540
  101.0 14.8 %all-to-all-start.1 = ((bf16[16,128,128]{2,1,0:T(8,128)(2,1)}), bf16[16,128,128]{2,1,0:T(8,128)(2,1)S(1)}, u32[]{:S(2)}, u32[]{:S(2)}) async-start(bf16[16,128,128]{2,1,0:T(8,128)(2,1)} %mixer.1), calls=%async_computation.1 | async-start | bytes 1048576 | tf_op jit(solution)/shard_map/all_to_all | solution.py:185
  105.5 137.7 %all-gather.2.cloned.1.call-start = ((), (), s32[]{:S(2)}) async-start(), calls=%async_computation.5 | async-start | bytes 18874368 | tf_op jit(solution)/shard_map/all_gather | solution.py:222
  117.6 4.3 copy-start.3
  121.8 5.8 %copy-start.4 = (f32[2048]{0:T(1024)S(1)}, f32[2048]{0:T(1024)}, u32[]{:S(2)}) copy-start(f32[2048]{0:T(1024)} %param.24) | copy-start | bytes 24580
  126.6 1.0 copy-start.1
  158.9 230.5 %reduce-scatter.2.cloned.1.call-start = ((), (), s32[]{:S(2)}) async-start(), calls=%async_computation.6 | async-start | bytes 18874368 | tf_op jit(solution)/shard_map/reduce_scatter | solution.py:227
  243.2 19.1 %copy-start.9 = (bf16[1,2048,640]{2,1,0:T(8,128)(2,1)S(1)}, bf16[1,2048,640]{2,1,0:T(8,128)(2,1)}, u32[]{:S(2)}) copy-start(bf16[1,2048,640]{2,1,0:T(8,128)(2,1)} %param.28) | copy-start | bytes 7864324
  297.8 102.6 %copy-start.7 = (f32[1,128,2]{1,2,0:T(2,128)S(1)}, f32[1,128,2]{1,2,0:T(2,128)}, u32[]{:S(2)}) copy-start(f32[1,128,2]{1,2,0:T(2,128)} %param.26) | copy-start | bytes 3076
  393.4 41.4 %all-to-all-start.3 = ((bf16[16,32,2048]{2,1,0:T(8,128)(2,1)}), bf16[16,32,2048]{2,1,0:T(8,128)(2,1)}, u32[]{:S(2)}, u32[]{:S(2)}) async-start(bf16[16,32,2048]{2,1,0:T(8,128)(2,1)} %copy.66), calls=%async_computation.4 | async-start | bytes 4194304 | tf_op jit(solution)/shard_map/all_to_all | solution.py:230
  443.4 4.9 %copy-start.2 = (f32[128,2048]{1,0:T(8,128)S(1)}, f32[128,2048]{1,0:T(8,128)}, u32[]{:S(2)}) copy-start(f32[128,2048]{1,0:T(8,128)} %copy-done.1) | copy-start | bytes 3145732
Sparse Core Ops, SparseCore 0:
  159.1 84.0 all-gather.1
  297.9 91.4 reduce-scatter.1
where the time goes:
time: 457 us; the launch traced here: 456 us
  waiting for transfers between devices  241 us (53%)
  matrix products  60 us (13%)
  Pallas kernels  48.4 us (11%)
  local copies, waits for them, and re-layouts  31 us (7%)
  blocking collectives  30.6 us (7%)
  starting transfers between devices  19.3 us (4%)
  between operations  13.6 us (3%)
  other arithmetic  12.5 us (3%)
    reduce_scatter x1, waiting for transfers between devices, body(): lax.psum_scatter(partial_value.astype(jnp.bfloat16), 'dp', scatter_dimens...  91.6 us
    all_gather x1, waiting for transfers between devices, body(): piece = lax.all_gather(arrived, 'dp', axis=0, tiled=True)  84 us
    pallas_call x1, Pallas kernels, mixer(): pl.pallas_call(mixer_kernel, out_shape=jax.ShapeDtypeStruct((n_blk, TOK,...  48.4 us
    all_to_all x1, waiting for transfers between devices, body(): lax.all_to_all(summed, 'sp', split_axis=0, concat_axis=0, tiled=True)  34.3 us
    all_to_all x1, blocking collectives, body(): lax.all_to_all(outgoing, 'sp', split_axis=0, concat_axis=0, tiled=True)  30.6 us
    all_to_all x1, waiting for transfers between devices, body(): lax.all_to_all(payload, 'sp', split_axis=0, concat_axis=0, tiled=True)  23.2 us
    dot_general x1, matrix products, expert_part(): up_act = jnp.dot(rows, up_local, preferred_element_type=jnp.float32)  19.5 us
    dot_general x1, matrix products, expert_part(): gate_act = jnp.dot(rows, gate_local, preferred_element_type=jnp.float32)  19.1 us
  transfers between devices with their start and end apart: 5, of which 5 were waited for; matrix products, arithmetic and copies ran while one was open for 1% of the time, Pallas kernels for 0%

commit v1 on v0

--- a/solution.py
+++ b/solution.py
@@ -127,29 +127,101 @@
     out_ref[...] = acc_ref[...].astype(jnp.bfloat16)
 
 
-def mixer(recv, rate, interpret=False):
+def in_vmem(count):
+    return [pl.BlockSpec(memory_space=pltpu.VMEM)] * count
+
+
+def mixer(recv, rate):
     n_blk = recv.shape[0]
     return pl.pallas_call(
         mixer_kernel,
         out_shape=jax.ShapeDtypeStruct((n_blk, TOK, HEAD_DIM), jnp.bfloat16),
-        in_specs=[pl.BlockSpec(memory_space=pltpu.VMEM)] * 2,
-        out_specs=pl.BlockSpec(memory_space=pltpu.VMEM),
+        in_specs=in_vmem(2),
+        out_specs=in_vmem(1)[0],
         scratch_shapes=[
             pltpu.VMEM((n_blk, 8, TOK), jnp.float32),
             pltpu.VMEM((2, n_blk, 2 * TOK, HEAD_DIM), jnp.bfloat16),
             pltpu.VMEM((2, n_blk, HEAD_DIM, HEAD_DIM), jnp.float32),
             pltpu.VMEM((n_blk, TOK, HEAD_DIM), jnp.float32),
         ],
+        compiler_params=pltpu.CompilerParams(vmem_limit_bytes=24 << 20),
+        cost_estimate=pl.CostEstimate(flops=20 * 10**9, bytes_accessed=3 << 20, transcendentals=0),
         name="mixer",
-        interpret=interpret,
     )(recv, rate)
 
 
-def expert_part(rows, gate_local, up_local, down_local):
-    gate_act = jnp.dot(rows, gate_local, preferred_element_type=jnp.float32)
-    up_act = jnp.dot(rows, up_local, preferred_element_type=jnp.float32)
-    hidden = (jax.nn.silu(gate_act) * up_act).astype(jnp.bfloat16)
-    return jnp.dot(hidden, down_local, preferred_element_type=jnp.float32)
+def pack_kernel(query_ref, key_ref, value_ref, logit_ref, out_ref):
+    logits = logit_ref[0].astype(jnp.float32).T.astype(jnp.bfloat16)
+    for h in range(out_ref.shape[0]):
+        lanes = slice(h * HEAD_DIM, (h + 1) * HEAD_DIM)
+        out_ref[h, 0:TOK, :] = query_ref[0, :, lanes]
+        out_ref[h, TOK : 2 * TOK, :] = key_ref[0, :, lanes]
+        out_ref[h, 2 * TOK : 3 * TOK, :] = value_ref[0, :, lanes]
+        out_ref[h, 3 * TOK :, :] = jnp.broadcast_to(logits[h : h + 1], (16, TOK))
+
+
+def packed_heads(query_proj, key_proj, value_proj, beta_logit):
+    n_heads = beta_logit.shape[2]
+    return pl.pallas_call(
+        pack_kernel,
+        out_shape=jax.ShapeDtypeStruct((n_heads, 3 * TOK + 16, HEAD_DIM), jnp.bfloat16),
+        in_specs=in_vmem(4),
+        out_specs=in_vmem(1)[0],
+        compiler_params=pltpu.CompilerParams(vmem_limit_bytes=16 << 20),
+        cost_estimate=pl.CostEstimate(flops=10**6, bytes_accessed=3 << 20, transcendentals=0),
+        name="pack",
+    )(query_proj, key_proj, value_proj, beta_logit)
+
+
+def expert_kernel(*refs, n_rows, n_parts):
+    rows, refs = refs[:n_rows], refs[n_rows:]
+    weights, refs = refs[: 3 * n_parts], refs[3 * n_parts :]
+    outs, refs = refs[:n_rows], refs[n_rows:]
+    bufs, accs, sems = refs[:3], refs[3 : 3 + n_rows], refs[3 + n_rows]
+    for s in range(n_parts):
+        for k in range(3):
+            pltpu.make_async_copy(weights[3 * s + k], bufs[k].at[s], sems.at[k, s]).start()
+    for acc in accs:
+        acc[...] = jnp.zeros(acc.shape, jnp.float32)
+
+    def part(s, carry):
+        for k in range(3):
+            pltpu.make_async_copy(weights[k], bufs[k].at[s], sems.at[k, s]).wait()
+        for r in range(n_rows):
+            gate_act = mm(rows[r][...], bufs[0][s])
+            up_act = mm(rows[r][...], bufs[1][s])
+            hidden = (jax.nn.silu(gate_act) * up_act).astype(jnp.bfloat16)
+            accs[r][...] += mm(hidden, bufs[2][s])
+        return carry
+
+    lax.fori_loop(0, n_parts, part, 0)
+    for acc, out in zip(accs, outs):
+        out[...] = acc[...].astype(jnp.bfloat16)
+
+
+def expert_part(rows, weights):
+    n_parts = len(weights)
+    count = sum(r.shape[0] for r in rows)
+    width, units = weights[0][0].shape
+    flat = [w for part in weights for w in part]
+    return pl.pallas_call(
+        lambda *refs: expert_kernel(*refs, n_rows=len(rows), n_parts=n_parts),
+        out_shape=[jax.ShapeDtypeStruct(r.shape, jnp.bfloat16) for r in rows],
+        in_specs=in_vmem(len(rows)) + [pl.BlockSpec(memory_space=pl.ANY)] * len(flat),
+        out_specs=in_vmem(len(rows)),
+        scratch_shapes=[pltpu.VMEM((n_parts, *w.shape), jnp.bfloat16) for w in weights[0]]
+        + [pltpu.VMEM(r.shape, jnp.float32) for r in rows]
+        + [pltpu.SemaphoreType.DMA((3, n_parts))],
+        compiler_params=pltpu.CompilerParams(vmem_limit_bytes=52 << 20),
+        cost_estimate=pl.CostEstimate(
+            flops=6 * count * width * units * n_parts,
+            bytes_accessed=6 * width * units * n_parts,
+            transcendentals=0,
+        ),
+    )(*rows, *flat)
+
+
+CHUNKS = 2
 
 
 def body(
@@ -169,28 +241,36 @@
     expert_up,
     expert_down,
 ):
-    tok_count = stream.shape[1]
-    model_width = stream.shape[2]
-    n_heads = beta_logit.shape[2]
-
-    def by_head(tensor):
-        return tensor[0].reshape(tok_count, n_heads, HEAD_DIM).transpose(1, 0, 2)
-
-    logits = jnp.pad(beta_logit[0].T[:, None, :], ((0, 0), (0, 15), (0, 0)))
-    payload = jnp.concatenate(
-        [by_head(query_proj), by_head(key_proj), by_head(value_proj), logits], axis=1
-    )
-    received = lax.all_to_all(payload, "sp", split_axis=0, concat_axis=0, tiled=True)
+    n_sp, n_dp = lax.axis_size("sp"), lax.axis_size("dp")
+    tok_count, model_width = stream.shape[1:]
+    chips = n_dp // 2
+    to_neighbour = []
+    for x in range(chips):
+        to_neighbour.append((2 * ((x + 1) % chips), 2 * x))
+        to_neighbour.append((2 * ((x - 1) % chips) + 1, 2 * x + 1))
+    to_core = [(i, i ^ 1) for i in range(n_dp)]
+    to_partner = [(i, (i + n_dp // 2) % n_dp) for i in range(n_dp)]
+
+    def over_sp(tensor):
+        return lax.all_to_all(tensor, "sp", split_axis=0, concat_axis=0, tiled=True)
+
+    own = (expert_gate[0], expert_up[0], expert_down[0])
+    near = tuple(lax.ppermute(w, "dp", to_core) for w in own)
+    far = tuple(lax.ppermute(w, "dp", to_neighbour) for w in own)
+    last = tuple(lax.ppermute(w, "dp", to_core) for w in far)
+    weights = (own, near, far, last)
+
+    received = over_sp(packed_heads(query_proj, key_proj, value_proj, beta_logit))
     mixed = mixer(received, log_decay.reshape(-1, TOK))
-    tokens_view = lax.all_to_all(mixed, "sp", split_axis=0, concat_axis=0, tiled=True)
-    per_head = tokens_view.astype(jnp.float32)
+    per_head = over_sp(mixed).astype(jnp.float32)
     normed_heads = (
         per_head
         * lax.rsqrt(jnp.mean(per_head * per_head, axis=-1, keepdims=True) + EPSILON)
         * head_gain
     )
     gated = (
-        normed_heads.transpose(1, 0, 2).reshape(tok_count, -1) * jax.nn.silu(out_gate[0].astype(jnp.float32))
+        normed_heads.transpose(1, 0, 2).reshape(tok_count, -1)
+        * jax.nn.silu(out_gate[0].astype(jnp.float32))
     ).astype(jnp.bfloat16)
     resid = stream[0].astype(jnp.float32) + jnp.dot(
         gated, out_proj, preferred_element_type=jnp.float32
@@ -198,40 +278,39 @@
     ffn_in = (
         resid * lax.rsqrt(jnp.mean(resid * resid, axis=-1, keepdims=True) + EPSILON) * ffn_gain
     ).astype(jnp.bfloat16)
-    n_sp = lax.axis_size("sp")
+
     top_count = routes.shape[2]
     capacity = tok_count * top_count * 2 // n_sp
+    piece = capacity // CHUNKS
     flat_routes = routes.reshape(-1)
     expert_ids = lax.broadcasted_iota(jnp.int32, (1, n_sp), 1)
     chosen = (flat_routes[:, None] == expert_ids).astype(jnp.int32)
     earlier = jnp.cumsum(chosen, axis=0) - chosen
-    slot_ids = flat_routes * capacity + jnp.sum(earlier * chosen, axis=1)
-    slot_grid = lax.broadcasted_iota(jnp.int32, (n_sp * capacity, 1), 0)
-    placing = (
-        (slot_grid == slot_ids[None, :])
-        .astype(jnp.int32)
-        .reshape(n_sp * capacity, tok_count, top_count)
-    )
-    placing = jnp.sum(placing, axis=2).astype(jnp.bfloat16)
+    place = jnp.sum(earlier * chosen, axis=1)
+    slot_ids = (place // piece) * (n_sp * piece) + flat_routes * piece + place % piece
+    slot_grid = lax.broadcasted_iota(jnp.int32, (n_sp * capacity, 1, 1), 0)
+    here = slot_grid == slot_ids.reshape(1, tok_count, top_count)
+    placing = jnp.sum(here.astype(jnp.int32), axis=2).astype(jnp.bfloat16)
+    share = jnp.sum(jnp.where(here, route_weight, 0.0), axis=2).T
+    share_high, share_low = halves(share)
     outgoing = jnp.dot(placing, ffn_in, preferred_element_type=jnp.float32).astype(jnp.bfloat16)
-    outgoing = outgoing.reshape(n_sp, capacity, model_width)
-    gate_local = expert_gate[0]
-    up_local = expert_up[0]
-    down_local = expert_down[0]
-    arrived = lax.all_to_all(outgoing, "sp", split_axis=0, concat_axis=0, tiled=True)
-    piece = lax.all_gather(arrived, "dp", axis=0, tiled=True)
-    flat_rows = piece.reshape(-1, model_width)
-    partial_value = expert_part(flat_rows, gate_local, up_local, down_local).reshape(
-        piece.shape[0], piece.shape[1], model_width
-    )
-    summed = lax.psum_scatter(
-        partial_value.astype(jnp.bfloat16), "dp", scatter_dimension=0, tiled=True
-    )
-    returned = lax.all_to_all(summed, "sp", split_axis=0, concat_axis=0, tiled=True)
-    picked = returned.reshape(n_sp * capacity, model_width)[slot_ids]
-    picked = picked.reshape(tok_count, top_count, model_width).astype(jnp.float32)
-    routed = jnp.sum(picked * route_weight[0][..., None], axis=1)
-    return (resid + routed).astype(jnp.bfloat16)[None]
+    outgoing = outgoing.reshape(CHUNKS, n_sp, piece, model_width)
+
+    mine, theirs = [], []
+    for c in range(CHUNKS):
+        arrived = over_sp(outgoing[c])
+        mine.append(arrived.reshape(-1, model_width))
+        theirs.append(lax.ppermute(arrived, "dp", to_partner).reshape(-1, model_width))
+    kept = expert_part(mine, weights)
+    result = resid
+    for c in range(CHUNKS):
+        (lent,) = expert_part([theirs[c]], weights)
+        back = lax.ppermute(lent, "dp", to_partner)
+        whole = (kept[c].astype(jnp.float32) + back.astype(jnp.float32)).astype(jnp.bfloat16)
+        home = over_sp(whole.reshape(n_sp, piece, model_width)).reshape(-1, model_width)
+        span = slice(c * n_sp * piece, (c + 1) * n_sp * piece)
+        result = result + mm(share_high[:, span], home) + mm(share_low[:, span], home)
+    return result.astype(jnp.bfloat16)[None]
 
 
 def solution(mesh):

time: 457 us -> 272 us (0.60)
  the two profiles are of different devices: /device:TPU:3 before, /device:TPU:0 now
where the time goes in v1:
time: 272 us; the launch traced here: 271 us
  Pallas kernels  105 us (39%)
  waiting for transfers between devices  78 us (29%)
  starting transfers between devices  45.6 us (17%)
  blocking collectives  21 us (8%)
  matrix products  7.86 us (3%)
  local copies, waits for them, and re-layouts  7.47 us (3%)
  other arithmetic  6 us (2%)
    all_to_all x5, waiting for transfers between devices, over_sp(): return lax.all_to_all(tensor, 'sp', split_axis=0, concat_axis=0, tiled=True)  65.9 us
    pallas_call x3, Pallas kernels, expert_part(): pl.pallas_call(lambda *refs: expert_kernel(*refs, n_rows=len(rows), n_par...  56.7 us
    pallas_call x1, Pallas kernels, mixer(): pl.pallas_call(mixer_kernel, out_shape=jax.ShapeDtypeStruct((n_blk, TOK,...  47 us
    all_to_all x5, starting transfers between devices, over_sp(): return lax.all_to_all(tensor, 'sp', split_axis=0, concat_axis=0, tiled=True)  27 us
    all_to_all x1, blocking collectives, over_sp(): return lax.all_to_all(tensor, 'sp', split_axis=0, concat_axis=0, tiled=True)  21 us
    ppermute x2, waiting for transfers between devices, body(): lax.ppermute(arrived, 'dp', to_partner).reshape(-1, model_width)  12 us
    ppermute x2, starting transfers between devices, body(): back = lax.ppermute(lent, 'dp', to_partner)  6.21 us
    ppermute x2, starting transfers between devices, body(): lax.ppermute(arrived, 'dp', to_partner).reshape(-1, model_width)  6.14 us
  transfers between devices with their start and end apart: 18, of which 7 were waited for; matrix products, arithmetic and copies ran while one was open for 6% of the time, Pallas kernels for 38%

profile of v1, /device:TPU:0, one launch (start us, length us, event | category | flops | bytes accessed | tf_op | source)
XLA Modules:
  0.0 271.3 jit_solution(16878643539000839560)
XLA Ops:
  5.4 8.2 %all-to-all-start = ((bf16[16,400,128]{2,1,0:T(8,128)(2,1)}), bf16[16,400,128]{2,1,0:T(8,128)(2,1)S(1)}, u32[]{:S(2)}, u32[]{:S(2)}) async-start(bf16[16,400,128]{2,1,0:T(8,128)(2,1)} %pack.1), calls=%async_computation | async-start | bytes 3276800 | tf_op jit(solution)/shard_map/all_to_all | solution.py:255
  13.7 2.8 %collective-permute-start.3 = (bf16[2048,640]{1,0:T(8,128)(2,1)}, bf16[2048,640]{1,0:T(8,128)(2,1)}, u32[]{:S(2)}, u32[]{:S(2)}) collective-permute-start(bf16[2048,640]{1,0:T(8,128)(2,1)} %bitcast.64), channel_id=1, source_target_pairs={{2,0},{7,1},{4,2},{1,3},{6,4},{3,5},{0,6},{5,7},{10,8},{15,9},{12,... | collective-permute-start | bytes 7864328 | tf_op jit(solution)/shard_map/ppermute | solution.py:259
  19.5 19.4 %all-to-all-done.recv_ref = bf16[16,400,128]{2,1,0:T(8,128)(2,1)S(1)} async-done(((bf16[16,400,128]{2,1,0:T(8,128)(2,1)}), bf16[16,400,128]{2,1,0:T(8,128)(2,1)S(1)}, u32[]{:S(2)}, u32[]{:S(2)}) %all-to-all-start) | async-done | bytes 1638432 | tf_op jit(solution)/shard_map/all_to_all | solution.py:255
  38.9 47.0 %mixer.1 = bf16[16,128,128]{2,1,0:T(8,128)(2,1)} custom-call(bf16[16,400,128]{2,1,0:T(8,128)(2,1)S(1)} %all-to-all-done.recv_ref, f32[16,128]{1,0:T(8,128)S(1)} %bitcast.62), custom_call_target="tpu_custom_call" | custom-call | flops 20000000000 | bytes 3145728 | tf_op jit(solution)/shard_map/mixer/pallas_call | solution.py:136
  85.9 3.7 %all-to-all-start.1 = ((bf16[16,128,128]{2,1,0:T(8,128)(2,1)}), bf16[16,128,128]{2,1,0:T(8,128)(2,1)S(1)}, u32[]{:S(2)}, u32[]{:S(2)}) async-start(bf16[16,128,128]{2,1,0:T(8,128)(2,1)} %mixer.1), calls=%async_computation.1 | async-start | bytes 1048576 | tf_op jit(solution)/shard_map/all_to_all | solution.py:255
  90.6 10.0 %all-to-all-done.1 = bf16[16,128,128]{2,1,0:T(8,128)(2,1)S(1)} async-done(((bf16[16,128,128]{2,1,0:T(8,128)(2,1)}), bf16[16,128,128]{2,1,0:T(8,128)(2,1)S(1)}, u32[]{:S(2)}, u32[]{:S(2)}) %all-to-all-start.1) | async-done | bytes 524320 | tf_op jit(solution)/shard_map/all_to_all | solution.py:255
  102.0 5.0 %multiply_reduce_fusion = (f32[128]{0:T(128)S(1)}, f32[128,2048]{1,0:T(8,128)S(1)}) fusion(bf16[128,2048]{0,1:T(8,128)(2,1)S(1)} %fusion.9, bf16[2048,2048]{1,0:T(8,128)(2,1)} %param.23, bf16[1,128,2048]{2,1,0:T(8,128)(2,1)} %param.15), kind=kOutput, calls=%fused_computation.22 | convolution fusion | flops 1074790272 | bytes 10486272 | tf_op jit(solution)/shard_map/dot_general | solution.py:275
  110.2 21.0 %all_to_all.30 = bf16[16,16,2048]{2,1,0:T(8,128)(2,1)} all-to-all(bf16[16,16,2048]{2,1,0:T(8,128)(2,1)S(1)} %bitcast.84), channel_id=1, replica_groups=mesh['sp'=16,'dp'=8] {'sp'}, dimensions={0} | all-to-all | bytes 2097152 | tf_op jit(solution)/shard_map/all_to_all | solution.py:255
  131.2 4.3 %all-to-all-start.3 = ((bf16[16,16,2048]{2,1,0:T(8,128)(2,1)}), bf16[16,16,2048]{2,1,0:T(8,128)(2,1)}, u32[]{:S(2)}, u32[]{:S(2)}) async-start(bf16[16,16,2048]{2,1,0:T(8,128)(2,1)} %bitcast.83), calls=%async_computation.3 | async-start | bytes 2097152 | tf_op jit(solution)/shard_map/all_to_all | solution.py:255
  135.6 3.1 %collective-permute-start.9 = (bf16[16,16,2048]{2,1,0:T(8,128)(2,1)}, bf16[16,16,2048]{2,1,0:T(8,128)(2,1)}, u32[]{:S(2)}, u32[]{:S(2)}) collective-permute-start(bf16[16,16,2048]{2,1,0:T(8,128)(2,1)} %all_to_all.30), channel_id=1, source_target_pairs={{0,4},{1,5},{2,6},{3,7},{4,0},{5,1},{6,2},{7,3},{8,12},{9,13},{10,... | collective-permute-start | bytes 3145736 | tf_op jit(solution)/shard_map/ppermute | solution.py:303
  138.7 13.8 %all-to-all-done.3 = bf16[16,16,2048]{2,1,0:T(8,128)(2,1)} async-done(((bf16[16,16,2048]{2,1,0:T(8,128)(2,1)}), bf16[16,16,2048]{2,1,0:T(8,128)(2,1)}, u32[]{:S(2)}, u32[]{:S(2)}) %all-to-all-start.3) | async-done | bytes 1048608 | tf_op jit(solution)/shard_map/all_to_all | solution.py:255
  152.5 3.0 %collective-permute-start.11 = (bf16[16,16,2048]{2,1,0:T(8,128)(2,1)}, bf16[16,16,2048]{2,1,0:T(8,128)(2,1)S(1)}, u32[]{:S(2)}, u32[]{:S(2)}) collective-permute-start(bf16[16,16,2048]{2,1,0:T(8,128)(2,1)} %all-to-all-done.3), channel_id=1, source_target_pairs={{0,4},{1,5},{2,6},{3,7},{4,0},{5,1},{6,2},{7,3},{8,12},{9,13},{10,... | collective-permute-start | bytes 3145736 | tf_op jit(solution)/shard_map/ppermute | solution.py:303
  155.5 8.0 %collective-permute-done.9 = bf16[16,16,2048]{2,1,0:T(8,128)(2,1)} collective-permute-done((bf16[16,16,2048]{2,1,0:T(8,128)(2,1)}, bf16[16,16,2048]{2,1,0:T(8,128)(2,1)}, u32[]{:S(2)}, u32[]{:S(2)}) %collective-permute-start.9) | collective-permute-done | bytes 1048608 | tf_op jit(solution)/shard_map/ppermute | solution.py:303
  163.5 15.2 %shard_map.146 = bf16[256,2048]{1,0:T(8,128)(2,1)S(1)} custom-call(bf16[256,2048]{1,0:T(8,128)(2,1)} %bitcast.17.refs_0_, bf16[2048,640]{1,0:T(8,128)(2,1)} %bitcast.65, bf16[2048,640]{1,0:T(8,128)(2,1)} %bitcast.70, bf16[640,2048]{1,0:T(8,128)(2,1)} %bitcast.74, bf16[2048,640]{1,0:T(8,128)(2,1)} %collective-permute-done.refs_5_.refs_4_, ...), custom_call_target="tpu_custom_call" | custom-call | flops 8053063680 | bytes 31457280 | tf_op jit(solution)/shard_map/pallas_call | solution.py:207
  178.7 3.1 %collective-permute-start.10 = (bf16[256,2048]{1,0:T(8,128)(2,1)S(1)}, bf16[256,2048]{1,0:T(8,128)(2,1)S(1)}, u32[]{:S(2)}, u32[]{:S(2)}) collective-permute-start(bf16[256,2048]{1,0:T(8,128)(2,1)S(1)} %shard_map.146), channel_id=1, source_target_pairs={{0,4},{1,5},{2,6},{3,7},{4,0},{5,1},{6,2},{7,3},{8,12},{9,13},{10,... | collective-permute-start | bytes 3145736 | tf_op jit(solution)/shard_map/ppermute | solution.py:308
  181.8 4.0 %collective-permute-done.11 = bf16[16,16,2048]{2,1,0:T(8,128)(2,1)S(1)} collective-permute-done((bf16[16,16,2048]{2,1,0:T(8,128)(2,1)}, bf16[16,16,2048]{2,1,0:T(8,128)(2,1)S(1)}, u32[]{:S(2)}, u32[]{:S(2)}) %collective-permute-start.11) | collective-permute-done | bytes 1048608 | tf_op jit(solution)/shard_map/ppermute | solution.py:303
  186.8 15.2 %shard_map.147 = bf16[256,2048]{1,0:T(8,128)(2,1)S(1)} custom-call(bf16[256,2048]{1,0:T(8,128)(2,1)} %bitcast.85, bf16[2048,640]{1,0:T(8,128)(2,1)} %bitcast.66, bf16[2048,640]{1,0:T(8,128)(2,1)} %bitcast.71, bf16[640,2048]{1,0:T(8,128)(2,1)} %bitcast.75, bf16[2048,640]{1,0:T(8,128)(2,1)} %collective-permute-done.refs_5_.refs_4_, ...), custom_call_target="tpu_custom_call" | custom-call | flops 8053063680 | bytes 31457280 | tf_op jit(solution)/shard_map/pallas_call | solution.py:207
  202.0 3.1 %collective-permute-start.12 = (bf16[256,2048]{1,0:T(8,128)(2,1)S(1)}, bf16[256,2048]{1,0:T(8,128)(2,1)S(1)}, u32[]{:S(2)}, u32[]{:S(2)}) collective-permute-start(bf16[256,2048]{1,0:T(8,128)(2,1)S(1)} %shard_map.147), channel_id=1, source_target_pairs={{0,4},{1,5},{2,6},{3,7},{4,0},{5,1},{6,2},{7,3},{8,12},{9,13},{10,... | collective-permute-start | bytes 3145736 | tf_op jit(solution)/shard_map/ppermute | solution.py:308
  205.2 26.3 %shard_map.145 = (bf16[256,2048]{1,0:T(8,128)(2,1)S(1)}, bf16[256,2048]{1,0:T(8,128)(2,1)}) custom-call(bf16[256,2048]{1,0:T(8,128)(2,1)} %bitcast.86, bf16[256,2048]{1,0:T(8,128)(2,1)} %bitcast.13.refs_1_, bf16[2048,640]{1,0:T(8,128)(2,1)} %bitcast.67, bf16[2048,640]{1,0:T(8,128)(2,1)} %bitcast.72, bf16[640,2048]{1,0:T(8,128)(2,1)} %bitcast.76, ...), custom_call_target="tpu_custom_call" | custom-call | flops 16106127360 | bytes 31457280 | tf_op jit(solution)/shard_map/pallas_call | solution.py:207
  232.8 7.1 %all-to-all-start.4 = ((bf16[16,16,2048]{2,1,0:T(8,128)(2,1)}), bf16[16,16,2048]{2,1,0:T(8,128)(2,1)S(1)}, u32[]{:S(2)}, u32[]{:S(2)}) async-start(bf16[16,16,2048]{2,1,0:T(8,128)(2,1)} %bitcast.18), calls=%async_computation.4 | async-start | bytes 2097152 | tf_op jit(solution)/shard_map/all_to_all | solution.py:255
  240.0 2.7 %add_convert_fusion = bf16[256,2048]{1,0:T(8,128)(2,1)} fusion(bf16[256,2048]{1,0:T(8,128)(2,1)S(1)} %collective-permute-done.12, bf16[256,2048]{1,0:T(8,128)(2,1)} %get-tuple-element.8), kind=kLoop, calls=%fused_computation.8 | loop fusion | flops 2097152 | bytes 3145728 | tf_op jit(solution)/shard_map/convert_element_type | solution.py:309
  242.7 10.3 %all-to-all-done.4 = bf16[16,16,2048]{2,1,0:T(8,128)(2,1)S(1)} async-done(((bf16[16,16,2048]{2,1,0:T(8,128)(2,1)}), bf16[16,16,2048]{2,1,0:T(8,128)(2,1)S(1)}, u32[]{:S(2)}, u32[]{:S(2)}) %all-to-all-start.4) | async-done | bytes 1048608 | tf_op jit(solution)/shard_map/all_to_all | solution.py:255
  253.0 3.7 %all-to-all-start.5 = ((bf16[16,16,2048]{2,1,0:T(8,128)(2,1)}), bf16[16,16,2048]{2,1,0:T(8,128)(2,1)S(1)}, u32[]{:S(2)}, u32[]{:S(2)}) async-start(bf16[16,16,2048]{2,1,0:T(8,128)(2,1)} %bitcast.82), calls=%async_computation.5 | async-start | bytes 2097152 | tf_op jit(solution)/shard_map/all_to_all | solution.py:255
  257.5 12.4 %all-to-all-done.5 = bf16[16,16,2048]{2,1,0:T(8,128)(2,1)S(1)} async-done(((bf16[16,16,2048]{2,1,0:T(8,128)(2,1)}), bf16[16,16,2048]{2,1,0:T(8,128)(2,1)S(1)}, u32[]{:S(2)}, u32[]{:S(2)}) %all-to-all-start.5) | async-done | bytes 1048608 | tf_op jit(solution)/shard_map/all_to_all | solution.py:255
  (76 shorter events, 18.6 us)
Async XLA Ops:
  3.9 14.7 %copy-start.10 = (s32[1,128,2]{1,2,0:T(2,128)S(1)}, s32[1,128,2]{1,2,0:T(2,128)}, u32[]{:S(2)}) copy-start(s32[1,128,2]{1,2,0:T(2,128)} %param.25) | copy-start | bytes 3076
  3.9 35.0 %copy-start.3 = (f32[1,1,2048]{2,1,0:T(1,128)S(1)}, f32[1,1,2048]{2,1,0:T(1,128)}, u32[]{:S(2)}) copy-start(f32[1,1,2048]{2,1,0:T(1,128)} %param.21) | copy-start | bytes 24580
  5.4 33.5 %all-to-all-start = ((bf16[16,400,128]{2,1,0:T(8,128)(2,1)}), bf16[16,400,128]{2,1,0:T(8,128)(2,1)S(1)}, u32[]{:S(2)}, u32[]{:S(2)}) async-start(bf16[16,400,128]{2,1,0:T(8,128)(2,1)} %pack.1), calls=%async_computation | async-start | bytes 3276800 | tf_op jit(solution)/shard_map/all_to_all | solution.py:255
  13.6 93.5 %collective-permute-start = (bf16[2048,640]{1,0:T(8,128)(2,1)}, bf16[2048,640]{1,0:T(8,128)(2,1)}, u32[]{:S(2)}, u32[]{:S(2)}) collective-permute-start(bf16[2048,640]{1,0:T(8,128)(2,1)} %bitcast.63), channel_id=1, source_target_pairs={{0,1},{1,0},{2,3},{3,2},{4,5},{5,4},{6,7},{7,6},{8,9},{9,8},{10,11... | collective-permute-start | bytes 7864328 | tf_op jit(solution)/shard_map/ppermute | solution.py:258
  13.7 94.3 %collective-permute-start.3 = (bf16[2048,640]{1,0:T(8,128)(2,1)}, bf16[2048,640]{1,0:T(8,128)(2,1)}, u32[]{:S(2)}, u32[]{:S(2)}) collective-permute-start(bf16[2048,640]{1,0:T(8,128)(2,1)} %bitcast.64), channel_id=1, source_target_pairs={{2,0},{7,1},{4,2},{1,3},{6,4},{3,5},{0,6},{5,7},{10,8},{15,9},{12,... | collective-permute-start | bytes 7864328 | tf_op jit(solution)/shard_map/ppermute | solution.py:259
  16.5 119.1 %collective-permute-start.1 = (bf16[2048,640]{1,0:T(8,128)(2,1)}, bf16[2048,640]{1,0:T(8,128)(2,1)}, u32[]{:S(2)}, u32[]{:S(2)}) collective-permute-start(bf16[2048,640]{1,0:T(8,128)(2,1)} %bitcast.68), channel_id=1, source_target_pairs={{0,1},{1,0},{2,3},{3,2},{4,5},{5,4},{6,7},{7,6},{8,9},{9,8},{10,11... | collective-permute-start | bytes 7864328 | tf_op jit(solution)/shard_map/ppermute | solution.py:258
  16.5 92.0 %collective-permute-start.4 = (bf16[2048,640]{1,0:T(8,128)(2,1)}, bf16[2048,640]{1,0:T(8,128)(2,1)}, u32[]{:S(2)}, u32[]{:S(2)}) collective-permute-start(bf16[2048,640]{1,0:T(8,128)(2,1)} %bitcast.69), channel_id=1, source_target_pairs={{2,0},{7,1},{4,2},{1,3},{6,4},{3,5},{0,6},{5,7},{10,8},{15,9},{12,... | collective-permute-start | bytes 7864328 | tf_op jit(solution)/shard_map/ppermute | solution.py:259
  17.3 91.3 %collective-permute-start.5 = (bf16[640,2048]{1,0:T(8,128)(2,1)}, bf16[640,2048]{1,0:T(8,128)(2,1)}, u32[]{:S(2)}, u32[]{:S(2)}) collective-permute-start(bf16[640,2048]{1,0:T(8,128)(2,1)} %bitcast.73), channel_id=1, source_target_pairs={{2,0},{7,1},{4,2},{1,3},{6,4},{3,5},{0,6},{5,7},{10,8},{15,9},{12,... | collective-permute-start | bytes 7864328 | tf_op jit(solution)/shard_map/ppermute | solution.py:259
  38.9 51.1 %copy-start.8 = (bf16[1,128,2048]{2,1,0:T(8,128)(2,1)S(1)}, bf16[1,128,2048]{2,1,0:T(8,128)(2,1)}, u32[]{:S(2)}) copy-start(bf16[1,128,2048]{2,1,0:T(8,128)(2,1)} %param.19) | copy-start | bytes 1572868
  85.9 15.2 %copy-start.12 = (f32[128]{0:T(128)S(1)}, f32[128]{0:T(128)}, u32[]{:S(2)}) copy-start(f32[128]{0:T(128)} %param.22) | copy-start | bytes 1540
  85.9 14.8 %all-to-all-start.1 = ((bf16[16,128,128]{2,1,0:T(8,128)(2,1)}), bf16[16,128,128]{2,1,0:T(8,128)(2,1)S(1)}, u32[]{:S(2)}, u32[]{:S(2)}) async-start(bf16[16,128,128]{2,1,0:T(8,128)(2,1)} %mixer.1), calls=%async_computation.1 | async-start | bytes 1048576 | tf_op jit(solution)/shard_map/all_to_all | solution.py:255
  107.0 31.7 %collective-permute-start.2 = (bf16[640,2048]{1,0:T(8,128)(2,1)S(1)}, bf16[640,2048]{1,0:T(8,128)(2,1)}, u32[]{:S(2)}, u32[]{:S(2)}) collective-permute-start(bf16[640,2048]{1,0:T(8,128)(2,1)S(1)} %bitcast.77), channel_id=1, source_target_pairs={{0,1},{1,0},{2,3},{3,2},{4,5},{5,4},{6,7},{7,6},{8,9},{9,8},{10,11... | collective-permute-start | bytes 7864328 | tf_op jit(solution)/shard_map/ppermute | solution.py:258
  107.9 55.6 %collective-permute-start.6 = (bf16[2048,640]{1,0:T(8,128)(2,1)}, bf16[2048,640]{1,0:T(8,128)(2,1)}, u32[]{:S(2)}, u32[]{:S(2)}) collective-permute-start(bf16[2048,640]{1,0:T(8,128)(2,1)} %collective-permute-done.3.refs_8_.refs_7_), channel_id=1, source_target_pairs={{0,1},{1,0},{2,3},{3,2},{4,5},{5,4},{6,7},{7,6},{8,9},{9,8},{10,11... | collective-permute-start | bytes 7864328 | tf_op jit(solution)/shard_map/ppermute | solution.py:260
  108.5 55.0 %collective-permute-start.7 = (bf16[2048,640]{1,0:T(8,128)(2,1)}, bf16[2048,640]{1,0:T(8,128)(2,1)}, u32[]{:S(2)}, u32[]{:S(2)}) collective-permute-start(bf16[2048,640]{1,0:T(8,128)(2,1)} %collective-permute-done.4.refs_9_.refs_8_), channel_id=1, source_target_pairs={{0,1},{1,0},{2,3},{3,2},{4,5},{5,4},{6,7},{7,6},{8,9},{9,8},{10,11... | collective-permute-start | bytes 7864328 | tf_op jit(solution)/shard_map/ppermute | solution.py:260
  108.6 54.9 %collective-permute-start.8 = (bf16[640,2048]{1,0:T(8,128)(2,1)}, bf16[640,2048]{1,0:T(8,128)(2,1)}, u32[]{:S(2)}, u32[]{:S(2)}) collective-permute-start(bf16[640,2048]{1,0:T(8,128)(2,1)} %collective-permute-done.5.refs_10_.refs_9_), channel_id=1, source_target_pairs={{0,1},{1,0},{2,3},{3,2},{4,5},{5,4},{6,7},{7,6},{8,9},{9,8},{10,11... | collective-permute-start | bytes 7864328 | tf_op jit(solution)/shard_map/ppermute | solution.py:260
  131.2 21.3 %all-to-all-start.3 = ((bf16[16,16,2048]{2,1,0:T(8,128)(2,1)}), bf16[16,16,2048]{2,1,0:T(8,128)(2,1)}, u32[]{:S(2)}, u32[]{:S(2)}) async-start(bf16[16,16,2048]{2,1,0:T(8,128)(2,1)} %bitcast.83), calls=%async_computation.3 | async-start | bytes 2097152 | tf_op jit(solution)/shard_map/all_to_all | solution.py:255
  135.6 27.9 %collective-permute-start.9 = (bf16[16,16,2048]{2,1,0:T(8,128)(2,1)}, bf16[16,16,2048]{2,1,0:T(8,128)(2,1)}, u32[]{:S(2)}, u32[]{:S(2)}) collective-permute-start(bf16[16,16,2048]{2,1,0:T(8,128)(2,1)} %all_to_all.30), channel_id=1, source_target_pairs={{0,4},{1,5},{2,6},{3,7},{4,0},{5,1},{6,2},{7,3},{8,12},{9,13},{10,... | collective-permute-start | bytes 3145736 | tf_op jit(solution)/shard_map/ppermute | solution.py:303
  152.5 33.4 %collective-permute-start.11 = (bf16[16,16,2048]{2,1,0:T(8,128)(2,1)}, bf16[16,16,2048]{2,1,0:T(8,128)(2,1)S(1)}, u32[]{:S(2)}, u32[]{:S(2)}) collective-permute-start(bf16[16,16,2048]{2,1,0:T(8,128)(2,1)} %all-to-all-done.3), channel_id=1, source_target_pairs={{0,4},{1,5},{2,6},{3,7},{4,0},{5,1},{6,2},{7,3},{8,12},{9,13},{10,... | collective-permute-start | bytes 3145736 | tf_op jit(solution)/shard_map/ppermute | solution.py:303
  178.7 52.7 %collective-permute-start.10 = (bf16[256,2048]{1,0:T(8,128)(2,1)S(1)}, bf16[256,2048]{1,0:T(8,128)(2,1)S(1)}, u32[]{:S(2)}, u32[]{:S(2)}) collective-permute-start(bf16[256,2048]{1,0:T(8,128)(2,1)S(1)} %shard_map.146), channel_id=1, source_target_pairs={{0,4},{1,5},{2,6},{3,7},{4,0},{5,1},{6,2},{7,3},{8,12},{9,13},{10,... | collective-permute-start | bytes 3145736 | tf_op jit(solution)/shard_map/ppermute | solution.py:308
  202.0 37.9 %collective-permute-start.12 = (bf16[256,2048]{1,0:T(8,128)(2,1)S(1)}, bf16[256,2048]{1,0:T(8,128)(2,1)S(1)}, u32[]{:S(2)}, u32[]{:S(2)}) collective-permute-start(bf16[256,2048]{1,0:T(8,128)(2,1)S(1)} %shard_map.147), channel_id=1, source_target_pairs={{0,4},{1,5},{2,6},{3,7},{4,0},{5,1},{6,2},{7,3},{8,12},{9,13},{10,... | collective-permute-start | bytes 3145736 | tf_op jit(solution)/shard_map/ppermute | solution.py:308
  232.8 20.2 %all-to-all-start.4 = ((bf16[16,16,2048]{2,1,0:T(8,128)(2,1)}), bf16[16,16,2048]{2,1,0:T(8,128)(2,1)S(1)}, u32[]{:S(2)}, u32[]{:S(2)}) async-start(bf16[16,16,2048]{2,1,0:T(8,128)(2,1)} %bitcast.18), calls=%async_computation.4 | async-start | bytes 2097152 | tf_op jit(solution)/shard_map/all_to_all | solution.py:255
  239.9 16.8 %copy-start.11 = (f32[1,128,2]{1,2,0:T(2,128)S(1)}, f32[1,128,2]{1,2,0:T(2,128)}, u32[]{:S(2)}) copy-start(f32[1,128,2]{1,2,0:T(2,128)} %param.26) | copy-start | bytes 3076
  239.9 16.9 %copy-start.6 = (f32[128,2048]{1,0:T(8,128)S(1)}, f32[128,2048]{1,0:T(8,128)}, u32[]{:S(2)}) copy-start(f32[128,2048]{1,0:T(8,128)} %copy-done.5) | copy-start | bytes 3145732
  253.0 16.8 %all-to-all-start.5 = ((bf16[16,16,2048]{2,1,0:T(8,128)(2,1)}), bf16[16,16,2048]{2,1,0:T(8,128)(2,1)S(1)}, u32[]{:S(2)}, u32[]{:S(2)}) async-start(bf16[16,16,2048]{2,1,0:T(8,128)(2,1)} %bitcast.82), calls=%async_computation.5 | async-start | bytes 2097152 | tf_op jit(solution)/shard_map/all_to_all | solution.py:255
  (7 other events, 17.4 us)

commit v2 on v1

--- a/solution.py
+++ b/solution.py
@@ -9,7 +9,7 @@
 HEAD_DIM = 128
 TOK = 128
 BASE = 16
-UNROLL = 2
+UNROLL = 4
 
 
 def mm(a, b):
@@ -27,26 +27,32 @@
     return mm(ah, bh) + (mm(ah, bl) + mm(al, bh))
 
 
-def unit_lower_inverse(low, rows, cols):
-    n = low.shape[0]
-    group = cols[:BASE] // BASE
-    packed = jnp.where(group == 0, low[:BASE], 0.0)
-    for b in range(1, n // BASE):
-        packed = packed + jnp.where(group == b, low[b * BASE : (b + 1) * BASE], 0.0)
-    inv = jnp.where(rows[:BASE] == cols[:BASE] % BASE, 1.0, 0.0)
+def unit_lower_inverses(lows, apart, cols):
+    n = cols.shape[0]
+    group = cols[:BASE] >> 4
+    packs, invs = [], []
+    for low in lows:
+        packed = jnp.where(group == 0, low[:BASE], 0.0)
+        for b in range(1, n // BASE):
+            packed = packed + jnp.where(group == b, low[b * BASE : (b + 1) * BASE], 0.0)
+        packs.append(packed)
+        invs.append(jnp.where(apart[:BASE] & (BASE - 1) == 0, 1.0, 0.0))
     for j in range(BASE - 1):
-        column = jnp.take_along_axis(packed, group * BASE + j, axis=1)
-        inv = inv - column * inv[j : j + 1]
-    full = jnp.concatenate([jnp.where(group == b, inv, 0.0) for b in range(n // BASE)], axis=0)
-    width = BASE
-    while width < n:
-        off = (rows // (2 * width) == cols // (2 * width)) & (rows // width != cols // width)
-        full = full - mm3(full, mm3(jnp.where(off, low, 0.0), full))
-        width *= 2
-    return full
-
-
-def mixer_kernel(recv_ref, rate_ref, out_ref, vec_ref, step_ref, add_ref, acc_ref):
+        columns = [jnp.take_along_axis(packed, (group << 4) + j, axis=1) for packed in packs]
+        invs = [inv - column * inv[j : j + 1] for inv, column in zip(invs, columns)]
+    fulls = [
+        jnp.concatenate([jnp.where(group == b, inv, 0.0) for b in range(n // BASE)], axis=0)
+        for inv in invs
+    ]
+    for shift in range(4, n.bit_length() - 1):
+        cross = apart >> shift == 1
+        firsts = [mm3(jnp.where(cross, low, 0.0), full) for low, full in zip(lows, fulls)]
+        seconds = [mm3(full, first) for full, first in zip(fulls, firsts)]
+        fulls = [full - second for full, second in zip(fulls, seconds)]
+    return fulls
+
+
+def mixer_kernel(recv_ref, rate_ref, out_ref, vec_ref, step_ref, lhs_ref, add_ref, acc_ref):
     n_blk = recv_ref.shape[0]
     rows = lax.broadcasted_iota(jnp.int32, (TOK, TOK), 0)
     cols = lax.broadcasted_iota(jnp.int32, (TOK, TOK), 1)
@@ -63,49 +69,63 @@
         vec_ref[n, 3:4, :] = jnp.broadcast_to(fwd_sum[n : n + 1, TOK - 1 : TOK], (1, TOK))
         vec_ref[n, 4:8, :] = jnp.zeros((4, TOK), jnp.float32)
 
-    def prepare(n):
-        query = recv_ref[n, 0:TOK, :]
-        key = recv_ref[n, TOK : 2 * TOK, :]
-        query_f = query.astype(jnp.float32)
-        key_f = key.astype(jnp.float32)
-        value_f = recv_ref[n, 2 * TOK : 3 * TOK, :].astype(jnp.float32)
-        key_tf = key_f.T
-        key_t = key_tf.astype(jnp.bfloat16)
-        key_c = lax.rsqrt(jnp.sum(key_f * key_f, axis=1, keepdims=True) + EPSILON)
-        key_r = lax.rsqrt(jnp.sum(key_tf * key_tf, axis=0, keepdims=True) + EPSILON)
-        query_c = lax.rsqrt(jnp.sum(query_f * query_f, axis=1, keepdims=True) + EPSILON) * HEAD_DIM ** (-0.5)
-        vec_r = vec_ref[n]
-        vec_c = vec_r.T
-        beta_r, beta_c = vec_r[2:3], vec_c[:, 2:3]
-        total = vec_r[3:4]
-        kk = mm(key, key_t) * key_c * key_r
-        qk = mm(query, key_t) * query_c * key_r
-        acc = None
-        for d in range(2):
-            sum_r, sum_c = vec_r[d : d + 1], vec_c[:, d : d + 1]
-            gap = sum_c - sum_r
-            if d == 0:
-                decay = jnp.exp(jnp.where(rows >= cols, gap, -jnp.inf))
-                low = jnp.where(rows > cols, kk * decay, 0.0) * beta_c
-                solve = unit_lower_inverse(low, rows, cols)
-            else:
-                decay = jnp.exp(jnp.where(rows <= cols, gap, -jnp.inf))
-                low = jnp.where(rows > cols, kk * jnp.exp(jnp.where(rows >= cols, -gap, -jnp.inf)), 0.0) * beta_r
-                solve = unit_lower_inverse(low, rows, cols).T
-            grown = jnp.exp(sum_c)
-            rhs = jnp.concatenate([value_f * beta_c, key_f * (beta_c * key_c * grown)], axis=1)
-            both = mm(solve.astype(jnp.bfloat16), rhs.astype(jnp.bfloat16)).astype(jnp.bfloat16)
-            lhs = jnp.concatenate([qk * decay, key_tf * (key_r * jnp.exp(total - sum_r))], axis=0)
-            done = mm(lhs.astype(jnp.bfloat16), both)
-            step_ref[d, n, 0:TOK, :] = (query_f * (query_c * grown) - done[:TOK, HEAD_DIM:]).astype(jnp.bfloat16)
-            step_ref[d, n, TOK:, :] = done[TOK:, HEAD_DIM:].astype(jnp.bfloat16)
-            add_ref[d, n] = done[TOK:, :HEAD_DIM]
-            acc = done[:TOK, :HEAD_DIM] if acc is None else acc + done[:TOK, :HEAD_DIM]
-        acc_ref[n] = acc
+    def prepare(blocks):
+        made, lows = [], []
+        for n in blocks:
+            query = recv_ref[n, 0:TOK, :]
+            key = recv_ref[n, TOK : 2 * TOK, :]
+            query_f = query.astype(jnp.float32)
+            key_f = key.astype(jnp.float32)
+            key_tf = key_f.T
+            key_t = key_tf.astype(jnp.bfloat16)
+            key_c = lax.rsqrt(jnp.sum(key_f * key_f, axis=1, keepdims=True) + EPSILON)
+            key_r = lax.rsqrt(jnp.sum(key_tf * key_tf, axis=0, keepdims=True) + EPSILON)
+            query_c = lax.rsqrt(jnp.sum(query_f * query_f, axis=1, keepdims=True) + EPSILON)
+            query_c = query_c * HEAD_DIM ** (-0.5)
+            vec_r = vec_ref[n]
+            vec_c = vec_r.T
+            kk = mm(key, key_t) * key_c * key_r
+            qk = mm(query, key_t) * query_c * key_r
+            for d in range(2):
+                sum_r, sum_c = vec_r[d : d + 1], vec_c[:, d : d + 1]
+                gap = sum_c - sum_r
+                if d == 0:
+                    decay = jnp.exp(jnp.where(rows >= cols, gap, -jnp.inf))
+                    lows.append(jnp.where(rows > cols, kk * decay, 0.0) * vec_c[:, 2:3])
+                else:
+                    decay = jnp.exp(jnp.where(rows <= cols, gap, -jnp.inf))
+                    turned = jnp.exp(jnp.where(rows >= cols, -gap, -jnp.inf))
+                    lows.append(jnp.where(rows > cols, kk * turned, 0.0) * vec_r[2:3])
+                lhs_ref[d, n, 0:TOK, :] = (qk * decay).astype(jnp.bfloat16)
+                tail = key_r * jnp.exp(vec_r[3:4] - sum_r)
+                lhs_ref[d, n, TOK:, :] = (key_tf * tail).astype(jnp.bfloat16)
+            made.append((key_c, query_c, vec_c))
+        solves = unit_lower_inverses(lows, rows ^ cols, cols)
+        boths = []
+        for i, n in enumerate(blocks):
+            key_c, query_c, vec_c = made[i]
+            beta_c = vec_c[:, 2:3]
+            key_f = recv_ref[n, TOK : 2 * TOK, :].astype(jnp.float32)
+            write = recv_ref[n, 2 * TOK : 3 * TOK, :].astype(jnp.float32) * beta_c
+            for d in range(2):
+                solve = solves[2 * i + d] if d == 0 else solves[2 * i + d].T
+                grown = jnp.exp(vec_c[:, d : d + 1])
+                rhs = jnp.concatenate([write, key_f * (beta_c * key_c * grown)], axis=1)
+                boths.append(mm(solve.astype(jnp.bfloat16), rhs.astype(jnp.bfloat16)).astype(jnp.bfloat16))
+        dones = [mm(lhs_ref[j % 2, blocks[j // 2]], both) for j, both in enumerate(boths)]
+        for i, n in enumerate(blocks):
+            key_c, query_c, vec_c = made[i]
+            query_f = recv_ref[n, 0:TOK, :].astype(jnp.float32)
+            for d in range(2):
+                done = dones[2 * i + d]
+                grown = query_c * jnp.exp(vec_c[:, d : d + 1])
+                step_ref[d, n, 0:TOK, :] = (query_f * grown - done[:TOK, HEAD_DIM:]).astype(jnp.bfloat16)
+                step_ref[d, n, TOK:, :] = done[TOK:, HEAD_DIM:].astype(jnp.bfloat16)
+                add_ref[d, n] = done[TOK:, :HEAD_DIM]
+            acc_ref[n] = dones[2 * i][:TOK, :HEAD_DIM] + dones[2 * i + 1][:TOK, :HEAD_DIM]
 
     def prepare_group(i, carry):
-        for u in range(UNROLL):
-            prepare(i * UNROLL + u)
+        prepare([i * UNROLL + u for u in range(UNROLL)])
         return carry
 
     lax.fori_loop(0, n_blk // UNROLL, prepare_group, 0)
@@ -141,6 +161,7 @@
         scratch_shapes=[
             pltpu.VMEM((n_blk, 8, TOK), jnp.float32),
             pltpu.VMEM((2, n_blk, 2 * TOK, HEAD_DIM), jnp.bfloat16),
+            pltpu.VMEM((2, n_blk, 2 * TOK, HEAD_DIM), jnp.bfloat16),
             pltpu.VMEM((2, n_blk, HEAD_DIM, HEAD_DIM), jnp.float32),
             pltpu.VMEM((n_blk, TOK, HEAD_DIM), jnp.float32),
         ],
@@ -173,9 +194,9 @@
     )(query_proj, key_proj, value_proj, beta_logit)
 
 
-def expert_kernel(*refs, n_rows, n_parts):
+def expert_kernel(*refs, n_rows, n_parts, n_after):
     rows, refs = refs[:n_rows], refs[n_rows:]
-    weights, refs = refs[: 3 * n_parts], refs[3 * n_parts :]
+    weights, refs = refs[: 3 * n_parts], refs[3 * n_parts + n_after :]
     outs, refs = refs[:n_rows], refs[n_rows:]
     bufs, accs, sems = refs[:3], refs[3 : 3 + n_rows], refs[3 + n_rows]
     for s in range(n_parts):
@@ -199,15 +220,15 @@
         out[...] = acc[...].astype(jnp.bfloat16)
 
 
-def expert_part(rows, weights):
+def expert_part(rows, weights, after=()):
     n_parts = len(weights)
     count = sum(r.shape[0] for r in rows)
     width, units = weights[0][0].shape
     flat = [w for part in weights for w in part]
     return pl.pallas_call(
-        lambda *refs: expert_kernel(*refs, n_rows=len(rows), n_parts=n_parts),
+        lambda *refs: expert_kernel(*refs, n_rows=len(rows), n_parts=n_parts, n_after=len(after)),
         out_shape=[jax.ShapeDtypeStruct(r.shape, jnp.bfloat16) for r in rows],
-        in_specs=in_vmem(len(rows)) + [pl.BlockSpec(memory_space=pl.ANY)] * len(flat),
+        in_specs=in_vmem(len(rows)) + [pl.BlockSpec(memory_space=pltpu.HBM)] * (len(flat) + len(after)),
         out_specs=in_vmem(len(rows)),
         scratch_shapes=[pltpu.VMEM((n_parts, *w.shape), jnp.bfloat16) for w in weights[0]]
         + [pltpu.VMEM(r.shape, jnp.float32) for r in rows]
@@ -218,7 +239,65 @@
             bytes_accessed=6 * width * units * n_parts,
             transcendentals=0,
         ),
-    )(*rows, *flat)
+    )(*rows, *flat, *after)
+
+
+def project_kernel(
+    mixed_ref, gate_ref, stream_ref, head_gain_ref, proj_hbm, ffn_gain_ref, placing_ref, *refs
+):
+    *outs, resid_ref, gated_ref, proj_ref, sems = refs
+    parts = sems.shape[0]
+    deep = proj_ref.shape[0] // parts
+    copies = []
+    for k in range(parts):
+        span = slice(k * deep, (k + 1) * deep)
+        copies.append(
+            pltpu.make_async_copy(proj_hbm.at[span, :], proj_ref.at[span, :], sems.at[k])
+        )
+        copies[-1].start()
+    for h in range(mixed_ref.shape[0]):
+        lanes = slice(h * HEAD_DIM, (h + 1) * HEAD_DIM)
+        head = mixed_ref[h].astype(jnp.float32)
+        scale = lax.rsqrt(jnp.mean(head * head, axis=1, keepdims=True) + EPSILON)
+        gate = jax.nn.silu(gate_ref[0, :, lanes].astype(jnp.float32))
+        gated_ref[:, lanes] = (head * scale * head_gain_ref[...] * gate).astype(jnp.bfloat16)
+    resid = stream_ref[0].astype(jnp.float32)
+    for k in range(parts):
+        span = slice(k * deep, (k + 1) * deep)
+        copies[k].wait()
+        resid = resid + mm(gated_ref[:, span], proj_ref[span, :])
+    resid_ref[...] = resid
+    scale = lax.rsqrt(jnp.mean(resid * resid, axis=1, keepdims=True) + EPSILON)
+    ffn_in = (resid * scale * ffn_gain_ref[...]).astype(jnp.bfloat16)
+    at = 0
+    for out in outs:
+        out[...] = mm(placing_ref[at : at + out.shape[0], :], ffn_in).astype(jnp.bfloat16)
+        at += out.shape[0]
+
+
+def project(mixed, out_gate, stream, head_gain, out_proj, ffn_gain, placing, n_out):
+    tok_count, model_width = stream.shape[1:]
+    part = placing.shape[0] // n_out
+    *outs, resid = pl.pallas_call(
+        project_kernel,
+        out_shape=[jax.ShapeDtypeStruct((part, model_width), jnp.bfloat16)] * n_out
+        + [jax.ShapeDtypeStruct((tok_count, model_width), jnp.float32)],
+        in_specs=in_vmem(4) + [pl.BlockSpec(memory_space=pltpu.HBM)] + in_vmem(2),
+        out_specs=in_vmem(n_out + 1),
+        scratch_shapes=[
+            pltpu.VMEM((tok_count, model_width), jnp.bfloat16),
+            pltpu.VMEM(out_proj.shape, jnp.bfloat16),
+            pltpu.SemaphoreType.DMA((4,)),
+        ],
+        compiler_params=pltpu.CompilerParams(vmem_limit_bytes=32 << 20),
+        cost_estimate=pl.CostEstimate(
+            flops=3 * tok_count * model_width * model_width,
+            bytes_accessed=2 * model_width * model_width,
+            transcendentals=0,
+        ),
+        name="project",
+    )(mixed, out_gate, stream, head_gain[None], out_proj, ffn_gain[None], placing)
+    return outs, resid
 
 
 CHUNKS = 2
@@ -257,28 +336,8 @@
     own = (expert_gate[0], expert_up[0], expert_down[0])
     near = tuple(lax.ppermute(w, "dp", to_core) for w in own)
     far = tuple(lax.ppermute(w, "dp", to_neighbour) for w in own)
-    last = tuple(lax.ppermute(w, "dp", to_core) for w in far)
-    weights = (own, near, far, last)
-
     received = over_sp(packed_heads(query_proj, key_proj, value_proj, beta_logit))
     mixed = mixer(received, log_decay.reshape(-1, TOK))
-    per_head = over_sp(mixed).astype(jnp.float32)
-    normed_heads = (
-        per_head
-        * lax.rsqrt(jnp.mean(per_head * per_head, axis=-1, keepdims=True) + EPSILON)
-        * head_gain
-    )
-    gated = (
-        normed_heads.transpose(1, 0, 2).reshape(tok_count, -1)
-        * jax.nn.silu(out_gate[0].astype(jnp.float32))
-    ).astype(jnp.bfloat16)
-    resid = stream[0].astype(jnp.float32) + jnp.dot(
-        gated, out_proj, preferred_element_type=jnp.float32
-    )
-    ffn_in = (
-        resid * lax.rsqrt(jnp.mean(resid * resid, axis=-1, keepdims=True) + EPSILON) * ffn_gain
-    ).astype(jnp.bfloat16)
-
     top_count = routes.shape[2]
     capacity = tok_count * top_count * 2 // n_sp
     piece = capacity // CHUNKS
@@ -293,20 +352,30 @@
     placing = jnp.sum(here.astype(jnp.int32), axis=2).astype(jnp.bfloat16)
     share = jnp.sum(jnp.where(here, route_weight, 0.0), axis=2).T
     share_high, share_low = halves(share)
-    outgoing = jnp.dot(placing, ffn_in, preferred_element_type=jnp.float32).astype(jnp.bfloat16)
-    outgoing = outgoing.reshape(CHUNKS, n_sp, piece, model_width)
+    outgoing, resid = project(
+        over_sp(mixed), out_gate, stream, head_gain, out_proj, ffn_gain, placing, CHUNKS
+    )
 
     mine, theirs = [], []
     for c in range(CHUNKS):
-        arrived = over_sp(outgoing[c])
+        arrived = over_sp(outgoing[c].reshape(n_sp, piece, model_width))
         mine.append(arrived.reshape(-1, model_width))
         theirs.append(lax.ppermute(arrived, "dp", to_partner).reshape(-1, model_width))
-    kept = expert_part(mine, weights)
+        if c == 0:
+            *far, mine[0] = lax.optimization_barrier((*far, mine[0]))
+            last = tuple(lax.ppermute(w, "dp", to_core) for w in far)
+    weights = (own, near, tuple(far), last)
+    turns = [("mine", 0)] + [("theirs", c) for c in range(CHUNKS)]
+    turns += [("mine", c) for c in range(1, CHUNKS)]
+    made, before = {}, ()
+    for side, c in turns:
+        rows = mine[c] if side == "mine" else theirs[c]
+        before = tuple(expert_part([rows], weights, before))
+        made[side, c] = before[0]
     result = resid
     for c in range(CHUNKS):
-        (lent,) = expert_part([theirs[c]], weights)
-        back = lax.ppermute(lent, "dp", to_partner)
-        whole = (kept[c].astype(jnp.float32) + back.astype(jnp.float32)).astype(jnp.bfloat16)
+        back = lax.ppermute(made["theirs", c], "dp", to_partner)
+        whole = (made["mine", c].astype(jnp.float32) + back.astype(jnp.float32)).astype(jnp.bfloat16)
         home = over_sp(whole.reshape(n_sp, piece, model_width)).reshape(-1, model_width)
         span = slice(c * n_sp * piece, (c + 1) * n_sp * piece)
         result = result + mm(share_high[:, span], home) + mm(share_low[:, span], home)

time: 272 us -> 237 us (0.87)
  the two profiles are of different devices: /device:TPU:0 before, /device:TPU:2 now
where the time goes in v2:
time: 237 us; the launch traced here: 236 us
  Pallas kernels  85.9 us (36%)
  waiting for transfers between devices  83.1 us (35%)
  starting transfers between devices  49.1 us (21%)
  local copies, waits for them, and re-layouts  10.9 us (5%)
  other arithmetic  4.91 us (2%)
    pallas_call x4, Pallas kernels, expert_part(): pl.pallas_call(lambda *refs: expert_kernel(*refs, n_rows=len(rows), n_par...  60.9 us
    all_to_all x6, waiting for transfers between devices, over_sp(): return lax.all_to_all(tensor, 'sp', split_axis=0, concat_axis=0, tiled=True)  59.3 us
    all_to_all x6, starting transfers between devices, over_sp(): return lax.all_to_all(tensor, 'sp', split_axis=0, concat_axis=0, tiled=True)  33.2 us
    pallas_call x1, Pallas kernels, mixer(): pl.pallas_call(mixer_kernel, out_shape=jax.ShapeDtypeStruct((n_blk, TOK,...  19.1 us
    ppermute x3, waiting for transfers between devices, body(): far = tuple((lax.ppermute(w, 'dp', to_neighbour) for w in own))  16.2 us
    unnamed x40, local copies, waits for them, and re-layouts  10.3 us
    ppermute x2, waiting for transfers between devices, body(): back = lax.ppermute(made['theirs', c], 'dp', to_partner)  7.57 us
    ppermute x2, starting transfers between devices, body(): lax.ppermute(arrived, 'dp', to_partner).reshape(-1, model_width)  6.75 us
  transfers between devices with their start and end apart: 19, of which 6 were waited for; matrix products, arithmetic and copies ran while one was open for 3% of the time, Pallas kernels for 36%

profile of v2, /device:TPU:2, one launch (start us, length us, event | category | flops | bytes accessed | tf_op | source)
XLA Modules:
  0.0 236.4 jit_solution(2913792463515256693)
XLA Ops:
  5.4 8.0 %all-to-all-start = ((bf16[16,400,128]{2,1,0:T(8,128)(2,1)}), bf16[16,400,128]{2,1,0:T(8,128)(2,1)S(1)}, u32[]{:S(2)}, u32[]{:S(2)}) async-start(bf16[16,400,128]{2,1,0:T(8,128)(2,1)} %pack.1), calls=%async_computation | async-start | bytes 3276800 | tf_op jit(solution)/shard_map/all_to_all | solution.py:334
  14.1 2.8 %collective-permute-start.1 = (bf16[2048,640]{1,0:T(8,128)(2,1)}, bf16[2048,640]{1,0:T(8,128)(2,1)}, u32[]{:S(2)}, u32[]{:S(2)}) collective-permute-start(bf16[2048,640]{1,0:T(8,128)(2,1)} %bitcast.59), channel_id=1, source_target_pairs={{2,0},{7,1},{4,2},{1,3},{6,4},{3,5},{0,6},{5,7},{10,8},{15,9},{12,... | collective-permute-start | bytes 7864328 | tf_op jit(solution)/shard_map/ppermute | solution.py:338
  18.6 20.2 %all-to-all-done.recv_ref = bf16[16,400,128]{2,1,0:T(8,128)(2,1)S(1)} async-done(((bf16[16,400,128]{2,1,0:T(8,128)(2,1)}), bf16[16,400,128]{2,1,0:T(8,128)(2,1)S(1)}, u32[]{:S(2)}, u32[]{:S(2)}) %all-to-all-start) | async-done | bytes 1638432 | tf_op jit(solution)/shard_map/all_to_all | solution.py:334
  38.8 19.1 %mixer.1 = bf16[16,128,128]{2,1,0:T(8,128)(2,1)S(1)} custom-call(bf16[16,400,128]{2,1,0:T(8,128)(2,1)S(1)} %all-to-all-done.recv_ref, f32[16,128]{1,0:T(8,128)S(1)} %bitcast.52), custom_call_target="tpu_custom_call" | custom-call | flops 20000000000 | bytes 3145728 | tf_op jit(solution)/shard_map/mixer/pallas_call | solution.py:156
  58.8 3.6 %all-to-all-start.1 = ((bf16[16,128,128]{2,1,0:T(8,128)(2,1)}), bf16[16,128,128]{2,1,0:T(8,128)(2,1)S(1)}, u32[]{:S(2)}, u32[]{:S(2)}) async-start(bf16[16,128,128]{2,1,0:T(8,128)(2,1)} %copy-done.10), calls=%async_computation.1 | async-start | bytes 1048576 | tf_op jit(solution)/shard_map/all_to_all | solution.py:334
  63.2 10.3 %all-to-all-done.1.mixed_ref = bf16[16,128,128]{2,1,0:T(8,128)(2,1)S(1)} async-done(((bf16[16,128,128]{2,1,0:T(8,128)(2,1)}), bf16[16,128,128]{2,1,0:T(8,128)(2,1)S(1)}, u32[]{:S(2)}, u32[]{:S(2)}) %all-to-all-start.1) | async-done | bytes 524320 | tf_op jit(solution)/shard_map/all_to_all | solution.py:334
  73.5 3.4 %copy-done.2 = bf16[2048,2048]{1,0:T(8,128)(2,1)S(1)} copy-done((bf16[2048,2048]{1,0:T(8,128)(2,1)S(1)}, bf16[2048,2048]{1,0:T(8,128)(2,1)}, u32[]{:S(2)}) %copy-start.2) | copy-done | bytes 8388632
  76.9 4.4 %project.1 = (bf16[256,2048]{1,0:T(8,128)(2,1)}, bf16[256,2048]{1,0:T(8,128)(2,1)}, f32[128,2048]{1,0:T(8,128)S(1)}) custom-call(bf16[16,128,128]{2,1,0:T(8,128)(2,1)S(1)} %all-to-all-done.1.mixed_ref, bf16[1,128,2048]{2,1,0:T(8,128)(2,1)S(1)} %copy-done.8, bf16[1,128,2048]{2,1,0:T(8,128)(2,1)S(1)} %copy-done.9, f32[1,128]{1,0:T(1,128)S(1)} %bitcast.51, ...), custom_call_target="tpu_custom_call" | custom-call | flops 1610612736 | bytes 8388608 | tf_op jit(solution)/shard_map/project/pallas_call | solution.py:281
  81.3 3.7 %all-to-all-start.2 = ((bf16[16,16,2048]{2,1,0:T(8,128)(2,1)}), bf16[16,16,2048]{2,1,0:T(8,128)(2,1)S(1)}, u32[]{:S(2)}, u32[]{:S(2)}) async-start(bf16[16,16,2048]{2,1,0:T(8,128)(2,1)} %bitcast.10), calls=%async_computation.2 | async-start | bytes 2097152 | tf_op jit(solution)/shard_map/all_to_all | solution.py:334
  85.6 16.2 %collective-permute-done.2.refs_9_ = bf16[640,2048]{1,0:T(8,128)(2,1)} collective-permute-done((bf16[640,2048]{1,0:T(8,128)(2,1)}, bf16[640,2048]{1,0:T(8,128)(2,1)}, u32[]{:S(2)}, u32[]{:S(2)}) %collective-permute-start.2) | collective-permute-done | bytes 2621472 | tf_op jit(solution)/shard_map/ppermute | solution.py:338
  102.4 7.1 %all-to-all-start.4 = ((bf16[16,16,2048]{2,1,0:T(8,128)(2,1)}), bf16[16,16,2048]{2,1,0:T(8,128)(2,1)S(1)}, u32[]{:S(2)}, u32[]{:S(2)}) async-start(bf16[16,16,2048]{2,1,0:T(8,128)(2,1)} %bitcast.15), calls=%async_computation.4 | async-start | bytes 2097152 | tf_op jit(solution)/shard_map/all_to_all | solution.py:334
  109.5 3.4 %collective-permute-start.9 = (bf16[16,16,2048]{2,1,0:T(8,128)(2,1)S(1)}, bf16[16,16,2048]{2,1,0:T(8,128)(2,1)}, u32[]{:S(2)}, u32[]{:S(2)}) collective-permute-start(bf16[16,16,2048]{2,1,0:T(8,128)(2,1)S(1)} %all-to-all-done.2), channel_id=1, source_target_pairs={{0,4},{1,5},{2,6},{3,7},{4,0},{5,1},{6,2},{7,3},{8,12},{9,13},{10,... | collective-permute-start | bytes 3145736 | tf_op jit(solution)/shard_map/ppermute | solution.py:363
  112.9 14.9 %all-to-all-done.4 = bf16[16,16,2048]{2,1,0:T(8,128)(2,1)S(1)} async-done(((bf16[16,16,2048]{2,1,0:T(8,128)(2,1)}), bf16[16,16,2048]{2,1,0:T(8,128)(2,1)S(1)}, u32[]{:S(2)}, u32[]{:S(2)}) %all-to-all-start.4) | async-done | bytes 1048608 | tf_op jit(solution)/shard_map/all_to_all | solution.py:334
  127.9 3.3 %collective-permute-start.11 = (bf16[16,16,2048]{2,1,0:T(8,128)(2,1)S(1)}, bf16[16,16,2048]{2,1,0:T(8,128)(2,1)S(1)}, u32[]{:S(2)}, u32[]{:S(2)}) collective-permute-start(bf16[16,16,2048]{2,1,0:T(8,128)(2,1)S(1)} %all-to-all-done.4), channel_id=1, source_target_pairs={{0,4},{1,5},{2,6},{3,7},{4,0},{5,1},{6,2},{7,3},{8,12},{9,13},{10,... | collective-permute-start | bytes 3145736 | tf_op jit(solution)/shard_map/ppermute | solution.py:363
  131.2 15.2 %shard_map.145.refs_13_ = bf16[256,2048]{1,0:T(8,128)(2,1)S(1)} custom-call(bf16[256,2048]{1,0:T(8,128)(2,1)} %bitcast.75, bf16[2048,640]{1,0:T(8,128)(2,1)} %bitcast.55, bf16[2048,640]{1,0:T(8,128)(2,1)} %bitcast.61, bf16[640,2048]{1,0:T(8,128)(2,1)} %bitcast.67, bf16[2048,640]{1,0:T(8,128)(2,1)} %collective-permute-done.3.refs_4_, ...), custom_call_target="tpu_custom_call" | custom-call | flops 8053063680 | bytes 31457280 | tf_op jit(solution)/shard_map/pallas_call | solution.py:228
  147.4 15.2 %shard_map.146.refs_13_ = bf16[256,2048]{1,0:T(8,128)(2,1)S(1)} custom-call(bf16[256,2048]{1,0:T(8,128)(2,1)} %bitcast.12.refs_0_, bf16[2048,640]{1,0:T(8,128)(2,1)} %bitcast.56, bf16[2048,640]{1,0:T(8,128)(2,1)} %bitcast.62, bf16[640,2048]{1,0:T(8,128)(2,1)} %bitcast.68, bf16[2048,640]{1,0:T(8,128)(2,1)} %collective-permute-done.3.refs_4_, ...), custom_call_target="tpu_custom_call" | custom-call | flops 8053063680 | bytes 31457280 | tf_op jit(solution)/shard_map/pallas_call | solution.py:228
  164.1 15.3 %shard_map.147.refs_13_ = bf16[256,2048]{1,0:T(8,128)(2,1)S(1)} custom-call(bf16[256,2048]{1,0:T(8,128)(2,1)} %bitcast.79, bf16[2048,640]{1,0:T(8,128)(2,1)} %bitcast.57, bf16[2048,640]{1,0:T(8,128)(2,1)} %bitcast.63, bf16[640,2048]{1,0:T(8,128)(2,1)} %bitcast.69, bf16[2048,640]{1,0:T(8,128)(2,1)} %collective-permute-done.3.refs_4_, ...), custom_call_target="tpu_custom_call" | custom-call | flops 8053063680 | bytes 31457280 | tf_op jit(solution)/shard_map/pallas_call | solution.py:228
  179.4 3.3 %collective-permute-start.12 = (bf16[256,2048]{1,0:T(8,128)(2,1)S(1)}, bf16[256,2048]{1,0:T(8,128)(2,1)}, u32[]{:S(2)}, u32[]{:S(2)}) collective-permute-start(bf16[256,2048]{1,0:T(8,128)(2,1)S(1)} %shard_map.147.refs_13_), channel_id=1, source_target_pairs={{0,4},{1,5},{2,6},{3,7},{4,0},{5,1},{6,2},{7,3},{8,12},{9,13},{10,... | collective-permute-start | bytes 3145736 | tf_op jit(solution)/shard_map/ppermute | solution.py:377
  182.7 7.6 %collective-permute-done.10 = bf16[256,2048]{1,0:T(8,128)(2,1)S(1)} collective-permute-done((bf16[256,2048]{1,0:T(8,128)(2,1)S(1)}, bf16[256,2048]{1,0:T(8,128)(2,1)S(1)}, u32[]{:S(2)}, u32[]{:S(2)}) %collective-permute-start.10) | collective-permute-done | bytes 1048608 | tf_op jit(solution)/shard_map/ppermute | solution.py:377
  191.6 3.7 %all-to-all-start.3 = ((bf16[16,16,2048]{2,1,0:T(8,128)(2,1)}), bf16[16,16,2048]{2,1,0:T(8,128)(2,1)S(1)}, u32[]{:S(2)}, u32[]{:S(2)}) async-start(bf16[16,16,2048]{2,1,0:T(8,128)(2,1)} %bitcast.77), calls=%async_computation.3 | async-start | bytes 2097152 | tf_op jit(solution)/shard_map/all_to_all | solution.py:334
  195.3 15.2 %shard_map.148 = bf16[256,2048]{1,0:T(8,128)(2,1)S(1)} custom-call(bf16[256,2048]{1,0:T(8,128)(2,1)} %bitcast.76, bf16[2048,640]{1,0:T(8,128)(2,1)} %bitcast.58, bf16[2048,640]{1,0:T(8,128)(2,1)} %bitcast.64, bf16[640,2048]{1,0:T(8,128)(2,1)} %bitcast.70, bf16[2048,640]{1,0:T(8,128)(2,1)} %collective-permute-done.3.refs_4_, ...), custom_call_target="tpu_custom_call" | custom-call | flops 8053063680 | bytes 31457280 | tf_op jit(solution)/shard_map/pallas_call | solution.py:228
  210.5 2.6 %add_convert_fusion = bf16[256,2048]{1,0:T(8,128)(2,1)} fusion(bf16[256,2048]{1,0:T(8,128)(2,1)} %collective-permute-done.12, bf16[256,2048]{1,0:T(8,128)(2,1)S(1)} %shard_map.148), kind=kLoop, calls=%fused_computation.6 | loop fusion | flops 2097152 | bytes 3145728 | tf_op jit(solution)/shard_map/convert_element_type | solution.py:378
  213.1 7.2 %all-to-all-start.5 = ((bf16[16,16,2048]{2,1,0:T(8,128)(2,1)}), bf16[16,16,2048]{2,1,0:T(8,128)(2,1)S(1)}, u32[]{:S(2)}, u32[]{:S(2)}) async-start(bf16[16,16,2048]{2,1,0:T(8,128)(2,1)} %bitcast.78), calls=%async_computation.5 | async-start | bytes 2097152 | tf_op jit(solution)/shard_map/all_to_all | solution.py:334
  221.1 13.9 %all-to-all-done.5 = bf16[16,16,2048]{2,1,0:T(8,128)(2,1)S(1)} async-done(((bf16[16,16,2048]{2,1,0:T(8,128)(2,1)}), bf16[16,16,2048]{2,1,0:T(8,128)(2,1)S(1)}, u32[]{:S(2)}, u32[]{:S(2)}) %all-to-all-start.5) | async-done | bytes 1048608 | tf_op jit(solution)/shard_map/all_to_all | solution.py:334
  (82 shorter events, 16.6 us)
Async XLA Ops:
  3.9 34.9 %copy-start.13 = (f32[1,1,2048]{2,1,0:T(1,128)S(1)}, f32[1,1,2048]{2,1,0:T(1,128)}, u32[]{:S(2)}) copy-start(f32[1,1,2048]{2,1,0:T(1,128)} %param.21) | copy-start | bytes 24580
  5.4 33.4 %all-to-all-start = ((bf16[16,400,128]{2,1,0:T(8,128)(2,1)}), bf16[16,400,128]{2,1,0:T(8,128)(2,1)S(1)}, u32[]{:S(2)}, u32[]{:S(2)}) async-start(bf16[16,400,128]{2,1,0:T(8,128)(2,1)} %pack.1), calls=%async_computation | async-start | bytes 3276800 | tf_op jit(solution)/shard_map/all_to_all | solution.py:334
  13.4 88.8 %collective-permute-start.3 = (bf16[2048,640]{1,0:T(8,128)(2,1)}, bf16[2048,640]{1,0:T(8,128)(2,1)}, u32[]{:S(2)}, u32[]{:S(2)}) collective-permute-start(bf16[2048,640]{1,0:T(8,128)(2,1)} %bitcast.53), channel_id=1, source_target_pairs={{0,1},{1,0},{2,3},{3,2},{4,5},{5,4},{6,7},{7,6},{8,9},{9,8},{10,11... | collective-permute-start | bytes 7864328 | tf_op jit(solution)/shard_map/ppermute | solution.py:337
  13.5 71.5 %collective-permute-start = (bf16[2048,640]{1,0:T(8,128)(2,1)}, bf16[2048,640]{1,0:T(8,128)(2,1)}, u32[]{:S(2)}, u32[]{:S(2)}) collective-permute-start(bf16[2048,640]{1,0:T(8,128)(2,1)} %bitcast.54), channel_id=1, source_target_pairs={{2,0},{7,1},{4,2},{1,3},{6,4},{3,5},{0,6},{5,7},{10,8},{15,9},{12,... | collective-permute-start | bytes 7864328 | tf_op jit(solution)/shard_map/ppermute | solution.py:338
  14.1 71.4 %collective-permute-start.1 = (bf16[2048,640]{1,0:T(8,128)(2,1)}, bf16[2048,640]{1,0:T(8,128)(2,1)}, u32[]{:S(2)}, u32[]{:S(2)}) collective-permute-start(bf16[2048,640]{1,0:T(8,128)(2,1)} %bitcast.59), channel_id=1, source_target_pairs={{2,0},{7,1},{4,2},{1,3},{6,4},{3,5},{0,6},{5,7},{10,8},{15,9},{12,... | collective-permute-start | bytes 7864328 | tf_op jit(solution)/shard_map/ppermute | solution.py:338
  16.9 84.9 %collective-permute-start.2 = (bf16[640,2048]{1,0:T(8,128)(2,1)}, bf16[640,2048]{1,0:T(8,128)(2,1)}, u32[]{:S(2)}, u32[]{:S(2)}) collective-permute-start(bf16[640,2048]{1,0:T(8,128)(2,1)} %bitcast.65), channel_id=1, source_target_pairs={{2,0},{7,1},{4,2},{1,3},{6,4},{3,5},{0,6},{5,7},{10,8},{15,9},{12,... | collective-permute-start | bytes 7864328 | tf_op jit(solution)/shard_map/ppermute | solution.py:338
  38.8 34.7 %copy-start.8 = (bf16[1,128,2048]{2,1,0:T(8,128)(2,1)S(1)}, bf16[1,128,2048]{2,1,0:T(8,128)(2,1)}, u32[]{:S(2)}) copy-start(bf16[1,128,2048]{2,1,0:T(8,128)(2,1)} %gate_ref.1) | copy-start | bytes 1572868
  38.8 34.7 %copy-start.9 = (bf16[1,128,2048]{2,1,0:T(8,128)(2,1)S(1)}, bf16[1,128,2048]{2,1,0:T(8,128)(2,1)}, u32[]{:S(2)}) copy-start(bf16[1,128,2048]{2,1,0:T(8,128)(2,1)} %stream_ref.1) | copy-start | bytes 1572868
  38.8 34.7 %copy-start.11 = (f32[2048]{0:T(1024)S(1)}, f32[2048]{0:T(1024)}, u32[]{:S(2)}) copy-start(f32[2048]{0:T(1024)} %param.24) | copy-start | bytes 24580
  38.8 34.7 %copy-start.12 = (f32[128]{0:T(128)S(1)}, f32[128]{0:T(128)}, u32[]{:S(2)}) copy-start(f32[128]{0:T(128)} %param.22) | copy-start | bytes 1540
  58.8 14.7 %all-to-all-start.1 = ((bf16[16,128,128]{2,1,0:T(8,128)(2,1)}), bf16[16,128,128]{2,1,0:T(8,128)(2,1)S(1)}, u32[]{:S(2)}, u32[]{:S(2)}) async-start(bf16[16,128,128]{2,1,0:T(8,128)(2,1)} %copy-done.10), calls=%async_computation.1 | async-start | bytes 1048576 | tf_op jit(solution)/shard_map/all_to_all | solution.py:334
  81.3 20.5 %all-to-all-start.2 = ((bf16[16,16,2048]{2,1,0:T(8,128)(2,1)}), bf16[16,16,2048]{2,1,0:T(8,128)(2,1)S(1)}, u32[]{:S(2)}, u32[]{:S(2)}) async-start(bf16[16,16,2048]{2,1,0:T(8,128)(2,1)} %bitcast.10), calls=%async_computation.2 | async-start | bytes 2097152 | tf_op jit(solution)/shard_map/all_to_all | solution.py:334
  85.0 24.5 %collective-permute-start.4 = (bf16[2048,640]{1,0:T(8,128)(2,1)}, bf16[2048,640]{1,0:T(8,128)(2,1)}, u32[]{:S(2)}, u32[]{:S(2)}) collective-permute-start(bf16[2048,640]{1,0:T(8,128)(2,1)} %bitcast.60), channel_id=1, source_target_pairs={{0,1},{1,0},{2,3},{3,2},{4,5},{5,4},{6,7},{7,6},{8,9},{9,8},{10,11... | collective-permute-start | bytes 7864328 | tf_op jit(solution)/shard_map/ppermute | solution.py:337
  85.1 27.8 %collective-permute-start.5 = (bf16[640,2048]{1,0:T(8,128)(2,1)}, bf16[640,2048]{1,0:T(8,128)(2,1)}, u32[]{:S(2)}, u32[]{:S(2)}) collective-permute-start(bf16[640,2048]{1,0:T(8,128)(2,1)} %bitcast.66), channel_id=1, source_target_pairs={{0,1},{1,0},{2,3},{3,2},{4,5},{5,4},{6,7},{7,6},{8,9},{9,8},{10,11... | collective-permute-start | bytes 7864328 | tf_op jit(solution)/shard_map/ppermute | solution.py:337
  101.8 29.4 %collective-permute-start.6 = (bf16[2048,640]{1,0:T(8,128)(2,1)}, bf16[2048,640]{1,0:T(8,128)(2,1)}, u32[]{:S(2)}, u32[]{:S(2)}) collective-permute-start(bf16[2048,640]{1,0:T(8,128)(2,1)} %collective-permute-done.refs_7_), channel_id=1, source_target_pairs={{0,1},{1,0},{2,3},{3,2},{4,5},{5,4},{6,7},{7,6},{8,9},{9,8},{10,11... | collective-permute-start | bytes 7864328 | tf_op jit(solution)/shard_map/ppermute | solution.py:366
  101.8 29.4 %collective-permute-start.7 = (bf16[2048,640]{1,0:T(8,128)(2,1)}, bf16[2048,640]{1,0:T(8,128)(2,1)}, u32[]{:S(2)}, u32[]{:S(2)}) collective-permute-start(bf16[2048,640]{1,0:T(8,128)(2,1)} %collective-permute-done.1.refs_8_), channel_id=1, source_target_pairs={{0,1},{1,0},{2,3},{3,2},{4,5},{5,4},{6,7},{7,6},{8,9},{9,8},{10,11... | collective-permute-start | bytes 7864328 | tf_op jit(solution)/shard_map/ppermute | solution.py:366
  102.3 28.9 %collective-permute-start.8 = (bf16[640,2048]{1,0:T(8,128)(2,1)}, bf16[640,2048]{1,0:T(8,128)(2,1)}, u32[]{:S(2)}, u32[]{:S(2)}) collective-permute-start(bf16[640,2048]{1,0:T(8,128)(2,1)} %collective-permute-done.2.refs_9_), channel_id=1, source_target_pairs={{0,1},{1,0},{2,3},{3,2},{4,5},{5,4},{6,7},{7,6},{8,9},{9,8},{10,11... | collective-permute-start | bytes 7864328 | tf_op jit(solution)/shard_map/ppermute | solution.py:366
  102.4 25.5 %all-to-all-start.4 = ((bf16[16,16,2048]{2,1,0:T(8,128)(2,1)}), bf16[16,16,2048]{2,1,0:T(8,128)(2,1)S(1)}, u32[]{:S(2)}, u32[]{:S(2)}) async-start(bf16[16,16,2048]{2,1,0:T(8,128)(2,1)} %bitcast.15), calls=%async_computation.4 | async-start | bytes 2097152 | tf_op jit(solution)/shard_map/all_to_all | solution.py:334
  109.5 37.9 %collective-permute-start.9 = (bf16[16,16,2048]{2,1,0:T(8,128)(2,1)S(1)}, bf16[16,16,2048]{2,1,0:T(8,128)(2,1)}, u32[]{:S(2)}, u32[]{:S(2)}) collective-permute-start(bf16[16,16,2048]{2,1,0:T(8,128)(2,1)S(1)} %all-to-all-done.2), channel_id=1, source_target_pairs={{0,4},{1,5},{2,6},{3,7},{4,0},{5,1},{6,2},{7,3},{8,12},{9,13},{10,... | collective-permute-start | bytes 3145736 | tf_op jit(solution)/shard_map/ppermute | solution.py:363
  127.9 35.2 %collective-permute-start.11 = (bf16[16,16,2048]{2,1,0:T(8,128)(2,1)S(1)}, bf16[16,16,2048]{2,1,0:T(8,128)(2,1)S(1)}, u32[]{:S(2)}, u32[]{:S(2)}) collective-permute-start(bf16[16,16,2048]{2,1,0:T(8,128)(2,1)S(1)} %all-to-all-done.4), channel_id=1, source_target_pairs={{0,4},{1,5},{2,6},{3,7},{4,0},{5,1},{6,2},{7,3},{8,12},{9,13},{10,... | collective-permute-start | bytes 3145736 | tf_op jit(solution)/shard_map/ppermute | solution.py:363
  162.6 27.6 %collective-permute-start.10 = (bf16[256,2048]{1,0:T(8,128)(2,1)S(1)}, bf16[256,2048]{1,0:T(8,128)(2,1)S(1)}, u32[]{:S(2)}, u32[]{:S(2)}) collective-permute-start(bf16[256,2048]{1,0:T(8,128)(2,1)S(1)} %shard_map.146.refs_13_), channel_id=1, source_target_pairs={{0,4},{1,5},{2,6},{3,7},{4,0},{5,1},{6,2},{7,3},{8,12},{9,13},{10,... | collective-permute-start | bytes 3145736 | tf_op jit(solution)/shard_map/ppermute | solution.py:377
  179.4 31.1 %collective-permute-start.12 = (bf16[256,2048]{1,0:T(8,128)(2,1)S(1)}, bf16[256,2048]{1,0:T(8,128)(2,1)}, u32[]{:S(2)}, u32[]{:S(2)}) collective-permute-start(bf16[256,2048]{1,0:T(8,128)(2,1)S(1)} %shard_map.147.refs_13_), channel_id=1, source_target_pairs={{0,4},{1,5},{2,6},{3,7},{4,0},{5,1},{6,2},{7,3},{8,12},{9,13},{10,... | collective-permute-start | bytes 3145736 | tf_op jit(solution)/shard_map/ppermute | solution.py:377
  191.6 21.5 %all-to-all-start.3 = ((bf16[16,16,2048]{2,1,0:T(8,128)(2,1)}), bf16[16,16,2048]{2,1,0:T(8,128)(2,1)S(1)}, u32[]{:S(2)}, u32[]{:S(2)}) async-start(bf16[16,16,2048]{2,1,0:T(8,128)(2,1)} %bitcast.77), calls=%async_computation.3 | async-start | bytes 2097152 | tf_op jit(solution)/shard_map/all_to_all | solution.py:334
  213.1 21.8 %all-to-all-start.5 = ((bf16[16,16,2048]{2,1,0:T(8,128)(2,1)}), bf16[16,16,2048]{2,1,0:T(8,128)(2,1)S(1)}, u32[]{:S(2)}, u32[]{:S(2)}) async-start(bf16[16,16,2048]{2,1,0:T(8,128)(2,1)} %bitcast.78), calls=%async_computation.5 | async-start | bytes 2097152 | tf_op jit(solution)/shard_map/all_to_all | solution.py:334
  (14 other events, 120.3 us)

commit v3 on v2

--- a/solution.py
+++ b/solution.py
@@ -5,11 +5,12 @@
 from jax.experimental.pallas import tpu as pltpu
 from jax.sharding import PartitionSpec as P
 
+
 EPSILON = 1e-6
 HEAD_DIM = 128
 TOK = 128
 BASE = 16
-UNROLL = 4
+UNROLL = 8
 
 
 def mm(a, b):
@@ -289,7 +290,7 @@
             pltpu.VMEM(out_proj.shape, jnp.bfloat16),
             pltpu.SemaphoreType.DMA((4,)),
         ],
-        compiler_params=pltpu.CompilerParams(vmem_limit_bytes=32 << 20),
+        compiler_params=pltpu.CompilerParams(vmem_limit_bytes=58 << 20),
         cost_estimate=pl.CostEstimate(
             flops=3 * tok_count * model_width * model_width,
             bytes_accessed=2 * model_width * model_width,
@@ -356,14 +357,13 @@
         over_sp(mixed), out_gate, stream, head_gain, out_proj, ffn_gain, placing, CHUNKS
     )
 
+    *far, outgoing[-1] = lax.optimization_barrier((*far, outgoing[-1]))
+    last = tuple(lax.ppermute(w, "dp", to_core) for w in far)
     mine, theirs = [], []
     for c in range(CHUNKS):
         arrived = over_sp(outgoing[c].reshape(n_sp, piece, model_width))
         mine.append(arrived.reshape(-1, model_width))
         theirs.append(lax.ppermute(arrived, "dp", to_partner).reshape(-1, model_width))
-        if c == 0:
-            *far, mine[0] = lax.optimization_barrier((*far, mine[0]))
-            last = tuple(lax.ppermute(w, "dp", to_core) for w in far)
     weights = (own, near, tuple(far), last)
     turns = [("mine", 0)] + [("theirs", c) for c in range(CHUNKS)]
     turns += [("mine", c) for c in range(1, CHUNKS)]

time: 237 us -> 257 us (1.084)
  blocking collectives: 0 us -> 25.1 us
  starting transfers between devices: 49.1 us -> 42.2 us
  local copies, waits for them, and re-layouts: 10.9 us -> 7.5 us
    all_to_all x0 -> x1, blocking collectives: none -> 25.1 us  [over_sp(): return lax.all_to_all(tensor, 'sp', split_axis=0, concat_axis=0, tiled=True)]
    all_to_all x6 -> x5, starting transfers between devices: 33.2 us -> 26.8 us  [over_sp(): return lax.all_to_all(tensor, 'sp', split_axis=0, concat_axis=0, tiled=True)]
    ppermute x3, waiting for transfers between devices: 16.2 us -> 21.6 us  [body(): far = tuple((lax.ppermute(w, 'dp', to_neighbour) for w in own))]
    all_to_all x6 -> x5, waiting for transfers between devices: 59.3 us -> 55.9 us  [over_sp(): return lax.all_to_all(tensor, 'sp', split_axis=0, concat_axis=0, tiled=True)]
    unnamed x40 -> x30, local copies, waits for them, and re-layouts: 10.3 us -> 6.84 us
    pallas_call x1, Pallas kernels: 4.42 us -> 7.67 us  [project(): pl.pallas_call(project_kernel, out_shape=[jax.ShapeDtypeStruct((part, mod...]
  transfers between devices with their start and end apart: 19 -> 18, of which waited for: 6 -> 6; matrix products, arithmetic and copies ran while one was open for 3% -> 3% of each run, Pallas kernels for 36% -> 34%
where the time goes in v3:
time: 257 us; the launch traced here: 256 us
  Pallas kernels  87.9 us (34%)
  waiting for transfers between devices  85.2 us (33%)
  starting transfers between devices  42.2 us (16%)
  blocking collectives  25.1 us (10%)
  local copies, waits for them, and re-layouts  7.5 us (3%)
  other arithmetic  5.67 us (2%)
    pallas_call x4, Pallas kernels, expert_part(): pl.pallas_call(lambda *refs: expert_kernel(*refs, n_rows=len(rows), n_par...  60.9 us
    all_to_all x5, waiting for transfers between devices, over_sp(): return lax.all_to_all(tensor, 'sp', split_axis=0, concat_axis=0, tiled=True)  55.9 us
    all_to_all x5, starting transfers between devices, over_sp(): return lax.all_to_all(tensor, 'sp', split_axis=0, concat_axis=0, tiled=True)  26.8 us
    all_to_all x1, blocking collectives, over_sp(): return lax.all_to_all(tensor, 'sp', split_axis=0, concat_axis=0, tiled=True)  25.1 us
    ppermute x3, waiting for transfers between devices, body(): far = tuple((lax.ppermute(w, 'dp', to_neighbour) for w in own))  21.6 us
    pallas_call x1, Pallas kernels, mixer(): pl.pallas_call(mixer_kernel, out_shape=jax.ShapeDtypeStruct((n_blk, TOK,...  17.9 us
    pallas_call x1, Pallas kernels, project(): pl.pallas_call(project_kernel, out_shape=[jax.ShapeDtypeStruct((part, mod...  7.67 us
    ppermute x2, waiting for transfers between devices, body(): back = lax.ppermute(made['theirs', c], 'dp', to_partner)  7.66 us
  transfers between devices with their start and end apart: 18, of which 6 were waited for; matrix products, arithmetic and copies ran while one was open for 3% of the time, Pallas kernels for 34%

profile of v3, /device:TPU:2, one launch (start us, length us, event | category | flops | bytes accessed | tf_op | source)
XLA Modules:
  0.0 256.0 jit_solution(2051325719273037977)
XLA Ops:
  3.9 1.4 pack.1
  5.4 8.0 %all-to-all-start = ((bf16[16,400,128]{2,1,0:T(8,128)(2,1)}), bf16[16,400,128]{2,1,0:T(8,128)(2,1)S(1)}, u32[]{:S(2)}, u32[]{:S(2)}) async-start(bf16[16,400,128]{2,1,0:T(8,128)(2,1)} %pack.1), calls=%async_computation | async-start | bytes 3276800 | tf_op jit(solution)/shard_map/all_to_all | solution.py:335
  15.2 1.7 collective-permute-start.4
  18.6 20.2 %all-to-all-done.recv_ref = bf16[16,400,128]{2,1,0:T(8,128)(2,1)S(1)} async-done(((bf16[16,400,128]{2,1,0:T(8,128)(2,1)}), bf16[16,400,128]{2,1,0:T(8,128)(2,1)S(1)}, u32[]{:S(2)}, u32[]{:S(2)}) %all-to-all-start) | async-done | bytes 1638432 | tf_op jit(solution)/shard_map/all_to_all | solution.py:335
  38.8 17.9 %mixer.1 = bf16[16,128,128]{2,1,0:T(8,128)(2,1)} custom-call(bf16[16,400,128]{2,1,0:T(8,128)(2,1)S(1)} %all-to-all-done.recv_ref, f32[16,128]{1,0:T(8,128)S(1)} %bitcast.50), custom_call_target="tpu_custom_call" | custom-call | flops 20000000000 | bytes 3145728 | tf_op jit(solution)/shard_map/mixer/pallas_call | solution.py:157
  56.7 3.6 %all-to-all-start.1 = ((bf16[16,128,128]{2,1,0:T(8,128)(2,1)}), bf16[16,128,128]{2,1,0:T(8,128)(2,1)S(1)}, u32[]{:S(2)}, u32[]{:S(2)}) async-start(bf16[16,128,128]{2,1,0:T(8,128)(2,1)} %mixer.1), calls=%async_computation.1 | async-start | bytes 1048576 | tf_op jit(solution)/shard_map/all_to_all | solution.py:335
  61.7 9.6 %all-to-all-done.1.mixed_ref = bf16[16,128,128]{2,1,0:T(8,128)(2,1)S(1)} async-done(((bf16[16,128,128]{2,1,0:T(8,128)(2,1)}), bf16[16,128,128]{2,1,0:T(8,128)(2,1)S(1)}, u32[]{:S(2)}, u32[]{:S(2)}) %all-to-all-start.1) | async-done | bytes 524320 | tf_op jit(solution)/shard_map/all_to_all | solution.py:335
  72.1 7.7 %project.1 = (bf16[256,2048]{1,0:T(8,128)(2,1)}, bf16[256,2048]{1,0:T(8,128)(2,1)}, f32[128,2048]{1,0:T(8,128)}) custom-call(bf16[16,128,128]{2,1,0:T(8,128)(2,1)} %copy-done.9, bf16[1,128,2048]{2,1,0:T(8,128)(2,1)} %gate_ref.1, bf16[1,128,2048]{2,1,0:T(8,128)(2,1)} %stream_ref.1, f32[1,128]{1,0:T(1,128)} %bitcast.79, bf16[2048,2048]{1,0:T(8,128)(2,1)} %proj_hbm.1, ...), custom_call_target="tpu_custom_call" | custom-call | flops 1610612736 | bytes 8388608 | tf_op jit(solution)/shard_map/project/pallas_call | solution.py:282
  80.1 21.6 %collective-permute-done.5.refs_9_ = bf16[640,2048]{1,0:T(8,128)(2,1)} collective-permute-done((bf16[640,2048]{1,0:T(8,128)(2,1)}, bf16[640,2048]{1,0:T(8,128)(2,1)}, u32[]{:S(2)}, u32[]{:S(2)}) %collective-permute-start.5) | collective-permute-done | bytes 2621472 | tf_op jit(solution)/shard_map/ppermute | solution.py:339
  102.3 25.1 %all_to_all.30 = bf16[16,16,2048]{2,1,0:T(8,128)(2,1)} all-to-all(bf16[16,16,2048]{2,1,0:T(8,128)(2,1)} %bitcast.76), channel_id=1, replica_groups=mesh['sp'=16,'dp'=8] {'sp'}, dimensions={0} | all-to-all | bytes 2097152 | tf_op jit(solution)/shard_map/all_to_all | solution.py:335
  127.4 4.3 %all-to-all-start.4 = ((bf16[16,16,2048]{2,1,0:T(8,128)(2,1)}), bf16[16,16,2048]{2,1,0:T(8,128)(2,1)}, u32[]{:S(2)}, u32[]{:S(2)}) async-start(bf16[16,16,2048]{2,1,0:T(8,128)(2,1)} %bitcast.75), calls=%async_computation.4 | async-start | bytes 2097152 | tf_op jit(solution)/shard_map/all_to_all | solution.py:335
  131.7 3.4 %collective-permute-start.9 = (bf16[16,16,2048]{2,1,0:T(8,128)(2,1)}, bf16[16,16,2048]{2,1,0:T(8,128)(2,1)}, u32[]{:S(2)}, u32[]{:S(2)}) collective-permute-start(bf16[16,16,2048]{2,1,0:T(8,128)(2,1)} %all_to_all.30), channel_id=1, source_target_pairs={{0,4},{1,5},{2,6},{3,7},{4,0},{5,1},{6,2},{7,3},{8,12},{9,13},{10,... | collective-permute-start | bytes 3145736 | tf_op jit(solution)/shard_map/ppermute | solution.py:366
  135.2 13.7 %all-to-all-done.4 = bf16[16,16,2048]{2,1,0:T(8,128)(2,1)} async-done(((bf16[16,16,2048]{2,1,0:T(8,128)(2,1)}), bf16[16,16,2048]{2,1,0:T(8,128)(2,1)}, u32[]{:S(2)}, u32[]{:S(2)}) %all-to-all-start.4) | async-done | bytes 1048608 | tf_op jit(solution)/shard_map/all_to_all | solution.py:335
  148.8 3.3 %collective-permute-start.11 = (bf16[16,16,2048]{2,1,0:T(8,128)(2,1)}, bf16[16,16,2048]{2,1,0:T(8,128)(2,1)S(1)}, u32[]{:S(2)}, u32[]{:S(2)}) collective-permute-start(bf16[16,16,2048]{2,1,0:T(8,128)(2,1)} %all-to-all-done.4), channel_id=1, source_target_pairs={{0,4},{1,5},{2,6},{3,7},{4,0},{5,1},{6,2},{7,3},{8,12},{9,13},{10,... | collective-permute-start | bytes 3145736 | tf_op jit(solution)/shard_map/ppermute | solution.py:366
  152.2 15.2 %shard_map.145.refs_13_ = bf16[256,2048]{1,0:T(8,128)(2,1)S(1)} custom-call(bf16[256,2048]{1,0:T(8,128)(2,1)} %bitcast.73, bf16[2048,640]{1,0:T(8,128)(2,1)} %bitcast.53, bf16[2048,640]{1,0:T(8,128)(2,1)} %bitcast.59, bf16[640,2048]{1,0:T(8,128)(2,1)} %bitcast.64, bf16[2048,640]{1,0:T(8,128)(2,1)} %collective-permute-done.refs_4_, ...), custom_call_target="tpu_custom_call" | custom-call | flops 8053063680 | bytes 31457280 | tf_op jit(solution)/shard_map/pallas_call | solution.py:229
  168.3 15.2 %shard_map.146.refs_13_ = bf16[256,2048]{1,0:T(8,128)(2,1)S(1)} custom-call(bf16[256,2048]{1,0:T(8,128)(2,1)} %bitcast.12.refs_0_, bf16[2048,640]{1,0:T(8,128)(2,1)} %bitcast.54, bf16[2048,640]{1,0:T(8,128)(2,1)} %bitcast.60, bf16[640,2048]{1,0:T(8,128)(2,1)} %bitcast.65, bf16[2048,640]{1,0:T(8,128)(2,1)} %collective-permute-done.refs_4_, ...), custom_call_target="tpu_custom_call" | custom-call | flops 8053063680 | bytes 31457280 | tf_op jit(solution)/shard_map/pallas_call | solution.py:229
  184.9 15.3 %shard_map.147.refs_13_ = bf16[256,2048]{1,0:T(8,128)(2,1)S(1)} custom-call(bf16[256,2048]{1,0:T(8,128)(2,1)} %bitcast.74, bf16[2048,640]{1,0:T(8,128)(2,1)} %bitcast.55, bf16[2048,640]{1,0:T(8,128)(2,1)} %bitcast.61, bf16[640,2048]{1,0:T(8,128)(2,1)} %bitcast.66, bf16[2048,640]{1,0:T(8,128)(2,1)} %collective-permute-done.refs_4_, ...), custom_call_target="tpu_custom_call" | custom-call | flops 8053063680 | bytes 31457280 | tf_op jit(solution)/shard_map/pallas_call | solution.py:229
  200.2 3.4 %collective-permute-start.12 = (bf16[256,2048]{1,0:T(8,128)(2,1)S(1)}, bf16[256,2048]{1,0:T(8,128)(2,1)}, u32[]{:S(2)}, u32[]{:S(2)}) collective-permute-start(bf16[256,2048]{1,0:T(8,128)(2,1)S(1)} %shard_map.147.refs_13_), channel_id=1, source_target_pairs={{0,4},{1,5},{2,6},{3,7},{4,0},{5,1},{6,2},{7,3},{8,12},{9,13},{10,... | collective-permute-start | bytes 3145736 | tf_op jit(solution)/shard_map/ppermute | solution.py:377
  203.5 7.7 %collective-permute-done.10 = bf16[256,2048]{1,0:T(8,128)(2,1)S(1)} collective-permute-done((bf16[256,2048]{1,0:T(8,128)(2,1)S(1)}, bf16[256,2048]{1,0:T(8,128)(2,1)S(1)}, u32[]{:S(2)}, u32[]{:S(2)}) %collective-permute-start.10) | collective-permute-done | bytes 1048608 | tf_op jit(solution)/shard_map/ppermute | solution.py:377
  212.5 3.9 %all-to-all-start.3 = ((bf16[16,16,2048]{2,1,0:T(8,128)(2,1)}), bf16[16,16,2048]{2,1,0:T(8,128)(2,1)S(1)}, u32[]{:S(2)}, u32[]{:S(2)}) async-start(bf16[16,16,2048]{2,1,0:T(8,128)(2,1)} %bitcast.13), calls=%async_computation.3 | async-start | bytes 2097152 | tf_op jit(solution)/shard_map/all_to_all | solution.py:335
  216.4 15.2 %shard_map.148 = bf16[256,2048]{1,0:T(8,128)(2,1)S(1)} custom-call(bf16[256,2048]{1,0:T(8,128)(2,1)} %bitcast.16.refs_0_, bf16[2048,640]{1,0:T(8,128)(2,1)} %bitcast.56, bf16[2048,640]{1,0:T(8,128)(2,1)} %bitcast.62, bf16[640,2048]{1,0:T(8,128)(2,1)} %bitcast.67, bf16[2048,640]{1,0:T(8,128)(2,1)} %collective-permute-done.refs_4_, ...), custom_call_target="tpu_custom_call" | custom-call | flops 8053063680 | bytes 31457280 | tf_op jit(solution)/shard_map/pallas_call | solution.py:229
  231.7 2.7 %add_convert_fusion = bf16[256,2048]{1,0:T(8,128)(2,1)} fusion(bf16[256,2048]{1,0:T(8,128)(2,1)} %collective-permute-done.12, bf16[256,2048]{1,0:T(8,128)(2,1)S(1)} %shard_map.148), kind=kLoop, calls=%fused_computation.6 | loop fusion | flops 2097152 | bytes 3145728 | tf_op jit(solution)/shard_map/convert_element_type | solution.py:378
  234.4 6.9 %all-to-all-start.5 = ((bf16[16,16,2048]{2,1,0:T(8,128)(2,1)}), bf16[16,16,2048]{2,1,0:T(8,128)(2,1)S(1)}, u32[]{:S(2)}, u32[]{:S(2)}) async-start(bf16[16,16,2048]{2,1,0:T(8,128)(2,1)} %bitcast.18), calls=%async_computation.5 | async-start | bytes 2097152 | tf_op jit(solution)/shard_map/all_to_all | solution.py:335
  242.1 12.3 %all-to-all-done.5 = bf16[16,16,2048]{2,1,0:T(8,128)(2,1)S(1)} async-done(((bf16[16,16,2048]{2,1,0:T(8,128)(2,1)}), bf16[16,16,2048]{2,1,0:T(8,128)(2,1)S(1)}, u32[]{:S(2)}, u32[]{:S(2)}) %all-to-all-start.5) | async-done | bytes 1048608 | tf_op jit(solution)/shard_map/all_to_all | solution.py:335
  (71 shorter events, 16.3 us)
Async XLA Ops:
  3.9 13.8 %copy-start.12 = (s32[1,128,2]{1,2,0:T(2,128)S(1)}, s32[1,128,2]{1,2,0:T(2,128)}, u32[]{:S(2)}) copy-start(s32[1,128,2]{1,2,0:T(2,128)} %param.25) | copy-start | bytes 3076
  3.9 34.9 %copy-start.7 = (f32[1,1,2048]{2,1,0:T(1,128)S(1)}, f32[1,1,2048]{2,1,0:T(1,128)}, u32[]{:S(2)}) copy-start(f32[1,1,2048]{2,1,0:T(1,128)} %param.21) | copy-start | bytes 24580
  5.4 33.4 %all-to-all-start = ((bf16[16,400,128]{2,1,0:T(8,128)(2,1)}), bf16[16,400,128]{2,1,0:T(8,128)(2,1)S(1)}, u32[]{:S(2)}, u32[]{:S(2)}) async-start(bf16[16,400,128]{2,1,0:T(8,128)(2,1)} %pack.1), calls=%async_computation | async-start | bytes 3276800 | tf_op jit(solution)/shard_map/all_to_all | solution.py:335
  13.4 88.8 %collective-permute-start = (bf16[2048,640]{1,0:T(8,128)(2,1)}, bf16[2048,640]{1,0:T(8,128)(2,1)}, u32[]{:S(2)}, u32[]{:S(2)}) collective-permute-start(bf16[2048,640]{1,0:T(8,128)(2,1)} %bitcast.51), channel_id=1, source_target_pairs={{0,1},{1,0},{2,3},{3,2},{4,5},{5,4},{6,7},{7,6},{8,9},{9,8},{10,11... | collective-permute-start | bytes 7864328 | tf_op jit(solution)/shard_map/ppermute | solution.py:338
  13.5 66.3 %collective-permute-start.3 = (bf16[2048,640]{1,0:T(8,128)(2,1)}, bf16[2048,640]{1,0:T(8,128)(2,1)}, u32[]{:S(2)}, u32[]{:S(2)}) collective-permute-start(bf16[2048,640]{1,0:T(8,128)(2,1)} %bitcast.52), channel_id=1, source_target_pairs={{2,0},{7,1},{4,2},{1,3},{6,4},{3,5},{0,6},{5,7},{10,8},{15,9},{12,... | collective-permute-start | bytes 7864328 | tf_op jit(solution)/shard_map/ppermute | solution.py:339
  14.1 117.6 %collective-permute-start.1 = (bf16[2048,640]{1,0:T(8,128)(2,1)}, bf16[2048,640]{1,0:T(8,128)(2,1)}, u32[]{:S(2)}, u32[]{:S(2)}) collective-permute-start(bf16[2048,640]{1,0:T(8,128)(2,1)} %bitcast.57), channel_id=1, source_target_pairs={{0,1},{1,0},{2,3},{3,2},{4,5},{5,4},{6,7},{7,6},{8,9},{9,8},{10,11... | collective-permute-start | bytes 7864328 | tf_op jit(solution)/shard_map/ppermute | solution.py:338
  15.2 64.9 %collective-permute-start.4 = (bf16[2048,640]{1,0:T(8,128)(2,1)}, bf16[2048,640]{1,0:T(8,128)(2,1)}, u32[]{:S(2)}, u32[]{:S(2)}) collective-permute-start(bf16[2048,640]{1,0:T(8,128)(2,1)} %bitcast.58), channel_id=1, source_target_pairs={{2,0},{7,1},{4,2},{1,3},{6,4},{3,5},{0,6},{5,7},{10,8},{15,9},{12,... | collective-permute-start | bytes 7864328 | tf_op jit(solution)/shard_map/ppermute | solution.py:339
  16.9 84.8 %collective-permute-start.5 = (bf16[640,2048]{1,0:T(8,128)(2,1)}, bf16[640,2048]{1,0:T(8,128)(2,1)}, u32[]{:S(2)}, u32[]{:S(2)}) collective-permute-start(bf16[640,2048]{1,0:T(8,128)(2,1)} %bitcast.63), channel_id=1, source_target_pairs={{2,0},{7,1},{4,2},{1,3},{6,4},{3,5},{0,6},{5,7},{10,8},{15,9},{12,... | collective-permute-start | bytes 7864328 | tf_op jit(solution)/shard_map/ppermute | solution.py:339
  56.7 14.7 %all-to-all-start.1 = ((bf16[16,128,128]{2,1,0:T(8,128)(2,1)}), bf16[16,128,128]{2,1,0:T(8,128)(2,1)S(1)}, u32[]{:S(2)}, u32[]{:S(2)}) async-start(bf16[16,128,128]{2,1,0:T(8,128)(2,1)} %mixer.1), calls=%async_computation.1 | async-start | bytes 1048576 | tf_op jit(solution)/shard_map/all_to_all | solution.py:335
  79.8 55.3 %collective-permute-start.2 = (bf16[640,2048]{1,0:T(8,128)(2,1)S(1)}, bf16[640,2048]{1,0:T(8,128)(2,1)}, u32[]{:S(2)}, u32[]{:S(2)}) collective-permute-start(bf16[640,2048]{1,0:T(8,128)(2,1)S(1)} %bitcast.68), channel_id=1, source_target_pairs={{0,1},{1,0},{2,3},{3,2},{4,5},{5,4},{6,7},{7,6},{8,9},{9,8},{10,11... | collective-permute-start | bytes 7864328 | tf_op jit(solution)/shard_map/ppermute | solution.py:338
  101.8 50.4 %collective-permute-start.6 = (bf16[2048,640]{1,0:T(8,128)(2,1)}, bf16[2048,640]{1,0:T(8,128)(2,1)}, u32[]{:S(2)}, u32[]{:S(2)}) collective-permute-start(bf16[2048,640]{1,0:T(8,128)(2,1)} %collective-permute-done.3.refs_7_), channel_id=1, source_target_pairs={{0,1},{1,0},{2,3},{3,2},{4,5},{5,4},{6,7},{7,6},{8,9},{9,8},{10,11... | collective-permute-start | bytes 7864328 | tf_op jit(solution)/shard_map/ppermute | solution.py:361
  101.8 50.4 %collective-permute-start.7 = (bf16[2048,640]{1,0:T(8,128)(2,1)}, bf16[2048,640]{1,0:T(8,128)(2,1)}, u32[]{:S(2)}, u32[]{:S(2)}) collective-permute-start(bf16[2048,640]{1,0:T(8,128)(2,1)} %collective-permute-done.4.refs_8_), channel_id=1, source_target_pairs={{0,1},{1,0},{2,3},{3,2},{4,5},{5,4},{6,7},{7,6},{8,9},{9,8},{10,11... | collective-permute-start | bytes 7864328 | tf_op jit(solution)/shard_map/ppermute | solution.py:361
  102.3 49.9 %collective-permute-start.8 = (bf16[640,2048]{1,0:T(8,128)(2,1)}, bf16[640,2048]{1,0:T(8,128)(2,1)}, u32[]{:S(2)}, u32[]{:S(2)}) collective-permute-start(bf16[640,2048]{1,0:T(8,128)(2,1)} %collective-permute-done.5.refs_9_), channel_id=1, source_target_pairs={{0,1},{1,0},{2,3},{3,2},{4,5},{5,4},{6,7},{7,6},{8,9},{9,8},{10,11... | collective-permute-start | bytes 7864328 | tf_op jit(solution)/shard_map/ppermute | solution.py:361
  127.4 21.4 %all-to-all-start.4 = ((bf16[16,16,2048]{2,1,0:T(8,128)(2,1)}), bf16[16,16,2048]{2,1,0:T(8,128)(2,1)}, u32[]{:S(2)}, u32[]{:S(2)}) async-start(bf16[16,16,2048]{2,1,0:T(8,128)(2,1)} %bitcast.75), calls=%async_computation.4 | async-start | bytes 2097152 | tf_op jit(solution)/shard_map/all_to_all | solution.py:335
  131.7 36.6 %collective-permute-start.9 = (bf16[16,16,2048]{2,1,0:T(8,128)(2,1)}, bf16[16,16,2048]{2,1,0:T(8,128)(2,1)}, u32[]{:S(2)}, u32[]{:S(2)}) collective-permute-start(bf16[16,16,2048]{2,1,0:T(8,128)(2,1)} %all_to_all.30), channel_id=1, source_target_pairs={{0,4},{1,5},{2,6},{3,7},{4,0},{5,1},{6,2},{7,3},{8,12},{9,13},{10,... | collective-permute-start | bytes 3145736 | tf_op jit(solution)/shard_map/ppermute | solution.py:366
  148.8 35.0 %collective-permute-start.11 = (bf16[16,16,2048]{2,1,0:T(8,128)(2,1)}, bf16[16,16,2048]{2,1,0:T(8,128)(2,1)S(1)}, u32[]{:S(2)}, u32[]{:S(2)}) collective-permute-start(bf16[16,16,2048]{2,1,0:T(8,128)(2,1)} %all-to-all-done.4), channel_id=1, source_target_pairs={{0,4},{1,5},{2,6},{3,7},{4,0},{5,1},{6,2},{7,3},{8,12},{9,13},{10,... | collective-permute-start | bytes 3145736 | tf_op jit(solution)/shard_map/ppermute | solution.py:366
  183.6 27.6 %collective-permute-start.10 = (bf16[256,2048]{1,0:T(8,128)(2,1)S(1)}, bf16[256,2048]{1,0:T(8,128)(2,1)S(1)}, u32[]{:S(2)}, u32[]{:S(2)}) collective-permute-start(bf16[256,2048]{1,0:T(8,128)(2,1)S(1)} %shard_map.146.refs_13_), channel_id=1, source_target_pairs={{0,4},{1,5},{2,6},{3,7},{4,0},{5,1},{6,2},{7,3},{8,12},{9,13},{10,... | collective-permute-start | bytes 3145736 | tf_op jit(solution)/shard_map/ppermute | solution.py:377
  184.9 26.3 %copy-start.1 = (bf16[256,2048]{1,0:T(8,128)(2,1)S(1)}, bf16[256,2048]{1,0:T(8,128)(2,1)}, u32[]{:S(2)}) copy-start(bf16[256,2048]{1,0:T(8,128)(2,1)} %copy-done) | copy-start | bytes 3145732
  200.1 12.4 %copy-start.2 = (bf16[256,2048]{1,0:T(8,128)(2,1)}, bf16[256,2048]{1,0:T(8,128)(2,1)S(1)}, u32[]{:S(2)}) copy-start(bf16[256,2048]{1,0:T(8,128)(2,1)S(1)} %shard_map.147.refs_13_) | copy-start | bytes 3145732
  200.2 31.5 %collective-permute-start.12 = (bf16[256,2048]{1,0:T(8,128)(2,1)S(1)}, bf16[256,2048]{1,0:T(8,128)(2,1)}, u32[]{:S(2)}, u32[]{:S(2)}) collective-permute-start(bf16[256,2048]{1,0:T(8,128)(2,1)S(1)} %shard_map.147.refs_13_), channel_id=1, source_target_pairs={{0,4},{1,5},{2,6},{3,7},{4,0},{5,1},{6,2},{7,3},{8,12},{9,13},{10,... | collective-permute-start | bytes 3145736 | tf_op jit(solution)/shard_map/ppermute | solution.py:377
  212.5 21.9 %all-to-all-start.3 = ((bf16[16,16,2048]{2,1,0:T(8,128)(2,1)}), bf16[16,16,2048]{2,1,0:T(8,128)(2,1)S(1)}, u32[]{:S(2)}, u32[]{:S(2)}) async-start(bf16[16,16,2048]{2,1,0:T(8,128)(2,1)} %bitcast.13), calls=%async_computation.3 | async-start | bytes 2097152 | tf_op jit(solution)/shard_map/all_to_all | solution.py:335
  231.6 9.7 %copy-start.13 = (f32[1,128,2]{1,2,0:T(2,128)S(1)}, f32[1,128,2]{1,2,0:T(2,128)}, u32[]{:S(2)}) copy-start(f32[1,128,2]{1,2,0:T(2,128)} %param.26) | copy-start | bytes 3076
  231.6 9.8 %copy-start.10 = (f32[128,2048]{1,0:T(8,128)S(1)}, f32[128,2048]{1,0:T(8,128)}, u32[]{:S(2)}) copy-start(f32[128,2048]{1,0:T(8,128)} %get-tuple-element.12) | copy-start | bytes 3145732
  234.4 20.1 %all-to-all-start.5 = ((bf16[16,16,2048]{2,1,0:T(8,128)(2,1)}), bf16[16,16,2048]{2,1,0:T(8,128)(2,1)S(1)}, u32[]{:S(2)}, u32[]{:S(2)}) async-start(bf16[16,16,2048]{2,1,0:T(8,128)(2,1)} %bitcast.18), calls=%async_computation.5 | async-start | bytes 2097152 | tf_op jit(solution)/shard_map/all_to_all | solution.py:335
  (8 other events, 14.5 us)

commit v4 on v3

--- a/solution.py
+++ b/solution.py
@@ -195,44 +195,46 @@
     )(query_proj, key_proj, value_proj, beta_logit)
 
 
-def expert_kernel(*refs, n_rows, n_parts, n_after):
-    rows, refs = refs[:n_rows], refs[n_rows:]
+def expert_kernel(rows, *refs, n_parts, n_after, n_out):
     weights, refs = refs[: 3 * n_parts], refs[3 * n_parts + n_after :]
-    outs, refs = refs[:n_rows], refs[n_rows:]
-    bufs, accs, sems = refs[:3], refs[3 : 3 + n_rows], refs[3 + n_rows]
+    outs, bufs, acc, sems = refs[:n_out], refs[n_out : n_out + 3], refs[n_out + 3], refs[n_out + 4]
     for s in range(n_parts):
         for k in range(3):
             pltpu.make_async_copy(weights[3 * s + k], bufs[k].at[s], sems.at[k, s]).start()
-    for acc in accs:
-        acc[...] = jnp.zeros(acc.shape, jnp.float32)
+    acc[...] = jnp.zeros(acc.shape, jnp.float32)
 
     def part(s, carry):
         for k in range(3):
             pltpu.make_async_copy(weights[k], bufs[k].at[s], sems.at[k, s]).wait()
-        for r in range(n_rows):
-            gate_act = mm(rows[r][...], bufs[0][s])
-            up_act = mm(rows[r][...], bufs[1][s])
-            hidden = (jax.nn.silu(gate_act) * up_act).astype(jnp.bfloat16)
-            accs[r][...] += mm(hidden, bufs[2][s])
+        gate_act = mm(rows[...], bufs[0][s])
+        up_act = mm(rows[...], bufs[1][s])
+        hidden = (jax.nn.silu(gate_act) * up_act).astype(jnp.bfloat16)
+        acc[...] += mm(hidden, bufs[2][s])
         return carry
 
     lax.fori_loop(0, n_parts, part, 0)
-    for acc, out in zip(accs, outs):
-        out[...] = acc[...].astype(jnp.bfloat16)
-
-
-def expert_part(rows, weights, after=()):
+    peers = outs[0].shape[0]
+    whole = acc[...].reshape(peers, acc.shape[0] // peers, acc.shape[1])
+    at = 0
+    for out in outs:
+        out[...] = whole[:, at : at + out.shape[1]].astype(jnp.bfloat16)
+        at += out.shape[1]
+
+
+def expert_part(rows, weights, peers, pieces, after=()):
     n_parts = len(weights)
-    count = sum(r.shape[0] for r in rows)
-    width, units = weights[0][0].shape
+    count, width = rows.shape
+    units = weights[0][0].shape[1]
     flat = [w for part in weights for w in part]
     return pl.pallas_call(
-        lambda *refs: expert_kernel(*refs, n_rows=len(rows), n_parts=n_parts, n_after=len(after)),
-        out_shape=[jax.ShapeDtypeStruct(r.shape, jnp.bfloat16) for r in rows],
-        in_specs=in_vmem(len(rows)) + [pl.BlockSpec(memory_space=pltpu.HBM)] * (len(flat) + len(after)),
-        out_specs=in_vmem(len(rows)),
+        lambda *refs: expert_kernel(
+            *refs, n_parts=n_parts, n_after=len(after), n_out=len(pieces)
+        ),
+        out_shape=[jax.ShapeDtypeStruct((peers, p, width), jnp.bfloat16) for p in pieces],
+        in_specs=in_vmem(1) + [pl.BlockSpec(memory_space=pltpu.HBM)] * (len(flat) + len(after)),
+        out_specs=in_vmem(len(pieces)),
         scratch_shapes=[pltpu.VMEM((n_parts, *w.shape), jnp.bfloat16) for w in weights[0]]
-        + [pltpu.VMEM(r.shape, jnp.float32) for r in rows]
+        + [pltpu.VMEM(rows.shape, jnp.float32)]
         + [pltpu.SemaphoreType.DMA((3, n_parts))],
         compiler_params=pltpu.CompilerParams(vmem_limit_bytes=52 << 20),
         cost_estimate=pl.CostEstimate(
@@ -240,7 +242,7 @@
             bytes_accessed=6 * width * units * n_parts,
             transcendentals=0,
         ),
-    )(*rows, *flat, *after)
+    )(rows, *flat, *after)
 
 
 def project_kernel(
@@ -351,7 +353,13 @@
     slot_grid = lax.broadcasted_iota(jnp.int32, (n_sp * capacity, 1, 1), 0)
     here = slot_grid == slot_ids.reshape(1, tok_count, top_count)
     placing = jnp.sum(here.astype(jnp.int32), axis=2).astype(jnp.bfloat16)
-    share = jnp.sum(jnp.where(here, route_weight, 0.0), axis=2).T
+    half = piece // 2
+    late = (place % piece) // half
+    home_ids = (CHUNKS - 1 + late) * (n_sp * half) + flat_routes * half + place % half
+    home_ids = (CHUNKS - 1) * (n_sp * half) + home_ids
+    home_ids = jnp.where(place // piece < CHUNKS - 1, slot_ids, home_ids)
+    there = slot_grid == home_ids.reshape(1, tok_count, top_count)
+    share = jnp.sum(jnp.where(there, route_weight, 0.0), axis=2).T
     share_high, share_low = halves(share)
     outgoing, resid = project(
         over_sp(mixed), out_gate, stream, head_gain, out_proj, ffn_gain, placing, CHUNKS
@@ -365,20 +373,24 @@
         mine.append(arrived.reshape(-1, model_width))
         theirs.append(lax.ppermute(arrived, "dp", to_partner).reshape(-1, model_width))
     weights = (own, near, tuple(far), last)
-    turns = [("mine", 0)] + [("theirs", c) for c in range(CHUNKS)]
-    turns += [("mine", c) for c in range(1, CHUNKS)]
+    pieces = [[piece]] * (CHUNKS - 1) + [[half, half]]
+    turns = [(side, c) for c in range(CHUNKS) for side in ("mine", "theirs")]
     made, before = {}, ()
     for side, c in turns:
         rows = mine[c] if side == "mine" else theirs[c]
-        before = tuple(expert_part([rows], weights, before))
-        made[side, c] = before[0]
-    result = resid
-    for c in range(CHUNKS):
-        back = lax.ppermute(made["theirs", c], "dp", to_partner)
-        whole = (made["mine", c].astype(jnp.float32) + back.astype(jnp.float32)).astype(jnp.bfloat16)
-        home = over_sp(whole.reshape(n_sp, piece, model_width)).reshape(-1, model_width)
-        span = slice(c * n_sp * piece, (c + 1) * n_sp * piece)
+        made[side, c] = expert_part(rows, weights, n_sp, pieces[c], before)
+        before = (made[side, c][0],)
+    kept = [out for c in range(CHUNKS) for out in made["mine", c]]
+    lent = [out for c in range(CHUNKS) for out in made["theirs", c]]
+    result, at = resid, 0
+    for c in range(len(kept)):
+        back = lax.ppermute(lent[c], "dp", to_partner)
+        whole = kept[c].astype(jnp.float32) + back.astype(jnp.float32)
+        whole = whole.astype(jnp.bfloat16)
+        home = over_sp(whole).reshape(-1, model_width)
+        span = slice(at, at + home.shape[0])
         result = result + mm(share_high[:, span], home) + mm(share_low[:, span], home)
+        at += home.shape[0]
     return result.astype(jnp.bfloat16)[None]
 
 

time: 257 us -> 273 us (1.062)
  the two profiles are of different devices: /device:TPU:2 before, /device:TPU:3 now
where the time goes in v4:
time: 273 us; the launch traced here: 269 us
  waiting for transfers between devices  89.8 us (33%)
  Pallas kernels  87.9 us (32%)
  starting transfers between devices  48.1 us (18%)
  blocking collectives  23.7 us (9%)
  local copies, waits for them, and re-layouts  8.4 us (3%)
  other arithmetic  7.63 us (3%)
  matrix products  2.74 us (1%)
    pallas_call x4, Pallas kernels, expert_part(): pl.pallas_call(lambda *refs: expert_kernel(*refs, n_parts=n_parts, n_afte...  60.9 us
    all_to_all x6, waiting for transfers between devices, over_sp(): return lax.all_to_all(tensor, 'sp', split_axis=0, concat_axis=0, tiled=True)  57.3 us
    all_to_all x6, starting transfers between devices, over_sp(): return lax.all_to_all(tensor, 'sp', split_axis=0, concat_axis=0, tiled=True)  30.8 us
    all_to_all x1, blocking collectives, over_sp(): return lax.all_to_all(tensor, 'sp', split_axis=0, concat_axis=0, tiled=True)  23.7 us
    ppermute x3, waiting for transfers between devices, body(): far = tuple((lax.ppermute(w, 'dp', to_neighbour) for w in own))  20.7 us
    pallas_call x1, Pallas kernels, mixer(): pl.pallas_call(mixer_kernel, out_shape=jax.ShapeDtypeStruct((n_blk, TOK,...  17.9 us
    ppermute x3, waiting for transfers between devices, body(): back = lax.ppermute(lent[c], 'dp', to_partner)  11.8 us
    unnamed x30, local copies, waits for them, and re-layouts  7.74 us
  transfers between devices with their start and end apart: 20, of which 8 were waited for; matrix products, arithmetic and copies ran while one was open for 4% of the time, Pallas kernels for 32%

profile of v4, /device:TPU:3, one launch (start us, length us, event | category | flops | bytes accessed | tf_op | source)
XLA Modules:
  0.0 268.6 jit_solution(8182886981083336410)
XLA Ops:
  5.4 7.8 %all-to-all-start = ((bf16[16,400,128]{2,1,0:T(8,128)(2,1)}), bf16[16,400,128]{2,1,0:T(8,128)(2,1)S(1)}, u32[]{:S(2)}, u32[]{:S(2)}) async-start(bf16[16,400,128]{2,1,0:T(8,128)(2,1)} %pack.1), calls=%async_computation | async-start | bytes 3276800 | tf_op jit(solution)/shard_map/all_to_all | solution.py:337
  18.1 19.0 %all-to-all-done.recv_ref = bf16[16,400,128]{2,1,0:T(8,128)(2,1)S(1)} async-done(((bf16[16,400,128]{2,1,0:T(8,128)(2,1)}), bf16[16,400,128]{2,1,0:T(8,128)(2,1)S(1)}, u32[]{:S(2)}, u32[]{:S(2)}) %all-to-all-start) | async-done | bytes 1638432 | tf_op jit(solution)/shard_map/all_to_all | solution.py:337
  37.2 17.9 %mixer.1 = bf16[16,128,128]{2,1,0:T(8,128)(2,1)} custom-call(bf16[16,400,128]{2,1,0:T(8,128)(2,1)S(1)} %all-to-all-done.recv_ref, f32[16,128]{1,0:T(8,128)S(1)} %bitcast.57), custom_call_target="tpu_custom_call" | custom-call | flops 20000000000 | bytes 3145728 | tf_op jit(solution)/shard_map/mixer/pallas_call | solution.py:157
  55.0 4.5 %all-to-all-start.1 = ((bf16[16,128,128]{2,1,0:T(8,128)(2,1)}), bf16[16,128,128]{2,1,0:T(8,128)(2,1)S(1)}, u32[]{:S(2)}, u32[]{:S(2)}) async-start(bf16[16,128,128]{2,1,0:T(8,128)(2,1)} %mixer.1), calls=%async_computation.1 | async-start | bytes 1048576 | tf_op jit(solution)/shard_map/all_to_all | solution.py:337
  61.0 8.9 %all-to-all-done.1.mixed_ref = bf16[16,128,128]{2,1,0:T(8,128)(2,1)S(1)} async-done(((bf16[16,128,128]{2,1,0:T(8,128)(2,1)}), bf16[16,128,128]{2,1,0:T(8,128)(2,1)S(1)}, u32[]{:S(2)}, u32[]{:S(2)}) %all-to-all-start.1) | async-done | bytes 524320 | tf_op jit(solution)/shard_map/all_to_all | solution.py:337
  70.6 7.7 %project.1 = (bf16[256,2048]{1,0:T(8,128)(2,1)}, bf16[256,2048]{1,0:T(8,128)(2,1)}, f32[128,2048]{1,0:T(8,128)}) custom-call(bf16[16,128,128]{2,1,0:T(8,128)(2,1)} %copy-done.8, bf16[1,128,2048]{2,1,0:T(8,128)(2,1)} %gate_ref.1, bf16[1,128,2048]{2,1,0:T(8,128)(2,1)} %stream_ref.1, f32[1,128]{1,0:T(1,128)} %bitcast.84, bf16[2048,2048]{1,0:T(8,128)(2,1)} %proj_hbm.1, ...), custom_call_target="tpu_custom_call" | custom-call | flops 1610612736 | bytes 8388608 | tf_op jit(solution)/shard_map/project/pallas_call | solution.py:284
  78.4 2.4 collective-permute-start.2
  80.8 20.7 %collective-permute-done.5.refs_9_ = bf16[640,2048]{1,0:T(8,128)(2,1)} collective-permute-done((bf16[640,2048]{1,0:T(8,128)(2,1)}, bf16[640,2048]{1,0:T(8,128)(2,1)}, u32[]{:S(2)}, u32[]{:S(2)}) %collective-permute-start.5) | collective-permute-done | bytes 2621472 | tf_op jit(solution)/shard_map/ppermute | solution.py:341
  103.0 23.7 %all_to_all.35 = bf16[16,16,2048]{2,1,0:T(8,128)(2,1)} all-to-all(bf16[16,16,2048]{2,1,0:T(8,128)(2,1)} %bitcast.81), channel_id=1, replica_groups=mesh['sp'=16,'dp'=8] {'sp'}, dimensions={0} | all-to-all | bytes 2097152 | tf_op jit(solution)/shard_map/all_to_all | solution.py:337
  126.6 4.3 %all-to-all-start.4 = ((bf16[16,16,2048]{2,1,0:T(8,128)(2,1)}), bf16[16,16,2048]{2,1,0:T(8,128)(2,1)}, u32[]{:S(2)}, u32[]{:S(2)}) async-start(bf16[16,16,2048]{2,1,0:T(8,128)(2,1)} %bitcast.80), calls=%async_computation.4 | async-start | bytes 2097152 | tf_op jit(solution)/shard_map/all_to_all | solution.py:337
  131.0 3.1 %collective-permute-start.9 = (bf16[16,16,2048]{2,1,0:T(8,128)(2,1)}, bf16[16,16,2048]{2,1,0:T(8,128)(2,1)}, u32[]{:S(2)}, u32[]{:S(2)}) collective-permute-start(bf16[16,16,2048]{2,1,0:T(8,128)(2,1)} %all_to_all.35), channel_id=1, source_target_pairs={{0,4},{1,5},{2,6},{3,7},{4,0},{5,1},{6,2},{7,3},{8,12},{9,13},{10,... | collective-permute-start | bytes 3145736 | tf_op jit(solution)/shard_map/ppermute | solution.py:374
  134.2 12.4 %all-to-all-done.4 = bf16[16,16,2048]{2,1,0:T(8,128)(2,1)} async-done(((bf16[16,16,2048]{2,1,0:T(8,128)(2,1)}), bf16[16,16,2048]{2,1,0:T(8,128)(2,1)}, u32[]{:S(2)}, u32[]{:S(2)}) %all-to-all-start.4) | async-done | bytes 1048608 | tf_op jit(solution)/shard_map/all_to_all | solution.py:337
  146.5 3.1 %collective-permute-start.11 = (bf16[16,16,2048]{2,1,0:T(8,128)(2,1)}, bf16[16,16,2048]{2,1,0:T(8,128)(2,1)S(1)}, u32[]{:S(2)}, u32[]{:S(2)}) collective-permute-start(bf16[16,16,2048]{2,1,0:T(8,128)(2,1)} %all-to-all-done.4), channel_id=1, source_target_pairs={{0,4},{1,5},{2,6},{3,7},{4,0},{5,1},{6,2},{7,3},{8,12},{9,13},{10,... | collective-permute-start | bytes 3145736 | tf_op jit(solution)/shard_map/ppermute | solution.py:374
  149.6 15.2 %shard_map.145.refs_13_ = bf16[16,16,2048]{2,1,0:T(8,128)(2,1)S(1)} custom-call(bf16[256,2048]{1,0:T(8,128)(2,1)} %bitcast.78, bf16[2048,640]{1,0:T(8,128)(2,1)} %bitcast.60, bf16[2048,640]{1,0:T(8,128)(2,1)} %bitcast.66, bf16[640,2048]{1,0:T(8,128)(2,1)} %bitcast.71, bf16[2048,640]{1,0:T(8,128)(2,1)} %collective-permute-done.refs_4_, ...), custom_call_target="tpu_custom_call" | custom-call | flops 8053063680 | bytes 31457280 | tf_op jit(solution)/shard_map/pallas_call | solution.py:229
  165.9 15.2 %shard_map.146.refs_13_ = bf16[16,16,2048]{2,1,0:T(8,128)(2,1)S(1)} custom-call(bf16[256,2048]{1,0:T(8,128)(2,1)} %bitcast.13.refs_0_, bf16[2048,640]{1,0:T(8,128)(2,1)} %bitcast.61, bf16[2048,640]{1,0:T(8,128)(2,1)} %bitcast.67, bf16[640,2048]{1,0:T(8,128)(2,1)} %bitcast.72, bf16[2048,640]{1,0:T(8,128)(2,1)} %collective-permute-done.refs_4_, ...), custom_call_target="tpu_custom_call" | custom-call | flops 8053063680 | bytes 31457280 | tf_op jit(solution)/shard_map/pallas_call | solution.py:229
  182.1 15.2 %shard_map.147 = (bf16[16,8,2048]{2,1,0:T(8,128)(2,1)S(1)}, bf16[16,8,2048]{2,1,0:T(8,128)(2,1)S(1)}) custom-call(bf16[256,2048]{1,0:T(8,128)(2,1)} %bitcast.16.refs_0_, bf16[2048,640]{1,0:T(8,128)(2,1)} %bitcast.62, bf16[2048,640]{1,0:T(8,128)(2,1)} %bitcast.68, bf16[640,2048]{1,0:T(8,128)(2,1)} %bitcast.73, ...), custom_call_target="tpu_custom_call" | custom-call | flops 8053063680 | bytes 31457280 | tf_op jit(solution)/shard_map/pallas_call | solution.py:229
  198.2 15.3 %shard_map.148 = (bf16[16,8,2048]{2,1,0:T(8,128)(2,1)S(1)}, bf16[16,8,2048]{2,1,0:T(8,128)(2,1)S(1)}) custom-call(bf16[256,2048]{1,0:T(8,128)(2,1)} %bitcast.79, bf16[2048,640]{1,0:T(8,128)(2,1)} %bitcast.63, bf16[2048,640]{1,0:T(8,128)(2,1)} %bitcast.69, bf16[640,2048]{1,0:T(8,128)(2,1)} %bitcast.74, bf16[2048,640]{1,0:T(8,128)(2,1)} %collective-permute-done.refs_4_, ...), custom_call_target="tpu_custom_call" | custom-call | flops 8053063680 | bytes 31457280 | tf_op jit(solution)/shard_map/pallas_call | solution.py:229
  218.0 4.2 %all-to-all-start.3 = ((bf16[16,16,2048]{2,1,0:T(8,128)(2,1)}), bf16[16,16,2048]{2,1,0:T(8,128)(2,1)S(1)}, u32[]{:S(2)}, u32[]{:S(2)}) async-start(bf16[16,16,2048]{2,1,0:T(8,128)(2,1)} %add_convert_fusion), calls=%async_computation.3 | async-start | bytes 2097152 | tf_op jit(solution)/shard_map/all_to_all | solution.py:337
  222.9 2.5 collective-permute-done.12
  227.4 9.3 %collective-permute-done.13 = bf16[16,8,2048]{2,1,0:T(8,128)(2,1)} collective-permute-done((bf16[16,8,2048]{2,1,0:T(8,128)(2,1)S(1)}, bf16[16,8,2048]{2,1,0:T(8,128)(2,1)}, u32[]{:S(2)}, u32[]{:S(2)}) %collective-permute-start.13) | collective-permute-done | bytes 524320 | tf_op jit(solution)/shard_map/ppermute | solution.py:387
  238.7 6.4 %all-to-all-start.5 = ((bf16[16,8,2048]{2,1,0:T(8,128)(2,1)}), bf16[16,8,2048]{2,1,0:T(8,128)(2,1)S(1)}, u32[]{:S(2)}, u32[]{:S(2)}) async-start(bf16[16,8,2048]{2,1,0:T(8,128)(2,1)} %add_convert_fusion.2), calls=%async_computation.5 | async-start | bytes 1048576 | tf_op jit(solution)/shard_map/all_to_all | solution.py:337
  245.9 8.8 %all-to-all-done.5 = bf16[16,8,2048]{2,1,0:T(8,128)(2,1)S(1)} async-done(((bf16[16,8,2048]{2,1,0:T(8,128)(2,1)}), bf16[16,8,2048]{2,1,0:T(8,128)(2,1)S(1)}, u32[]{:S(2)}, u32[]{:S(2)}) %all-to-all-start.5) | async-done | bytes 524320 | tf_op jit(solution)/shard_map/all_to_all | solution.py:337
  254.7 3.6 %all-to-all-start.6 = ((bf16[16,8,2048]{2,1,0:T(8,128)(2,1)}), bf16[16,8,2048]{2,1,0:T(8,128)(2,1)S(1)}, u32[]{:S(2)}, u32[]{:S(2)}) async-start(bf16[16,8,2048]{2,1,0:T(8,128)(2,1)} %add_convert_fusion.1), calls=%async_computation.6 | async-start | bytes 1048576 | tf_op jit(solution)/shard_map/all_to_all | solution.py:337
  258.9 8.3 %all-to-all-done.6 = bf16[16,8,2048]{2,1,0:T(8,128)(2,1)S(1)} async-done(((bf16[16,8,2048]{2,1,0:T(8,128)(2,1)}), bf16[16,8,2048]{2,1,0:T(8,128)(2,1)S(1)}, u32[]{:S(2)}, u32[]{:S(2)}) %all-to-all-start.6) | async-done | bytes 524320 | tf_op jit(solution)/shard_map/all_to_all | solution.py:337
  (78 shorter events, 28.9 us)
Async XLA Ops:
  3.9 33.2 %copy-start.6 = (f32[1,1,2048]{2,1,0:T(1,128)S(1)}, f32[1,1,2048]{2,1,0:T(1,128)}, u32[]{:S(2)}) copy-start(f32[1,1,2048]{2,1,0:T(1,128)} %param.21) | copy-start | bytes 24580
  5.4 31.8 %all-to-all-start = ((bf16[16,400,128]{2,1,0:T(8,128)(2,1)}), bf16[16,400,128]{2,1,0:T(8,128)(2,1)S(1)}, u32[]{:S(2)}, u32[]{:S(2)}) async-start(bf16[16,400,128]{2,1,0:T(8,128)(2,1)} %pack.1), calls=%async_computation | async-start | bytes 3276800 | tf_op jit(solution)/shard_map/all_to_all | solution.py:337
  13.2 89.3 %collective-permute-start = (bf16[2048,640]{1,0:T(8,128)(2,1)}, bf16[2048,640]{1,0:T(8,128)(2,1)}, u32[]{:S(2)}, u32[]{:S(2)}) collective-permute-start(bf16[2048,640]{1,0:T(8,128)(2,1)} %bitcast.58), channel_id=1, source_target_pairs={{0,1},{1,0},{2,3},{3,2},{4,5},{5,4},{6,7},{7,6},{8,9},{9,8},{10,11... | collective-permute-start | bytes 7864328 | tf_op jit(solution)/shard_map/ppermute | solution.py:340
  14.2 64.2 %collective-permute-start.3 = (bf16[2048,640]{1,0:T(8,128)(2,1)}, bf16[2048,640]{1,0:T(8,128)(2,1)}, u32[]{:S(2)}, u32[]{:S(2)}) collective-permute-start(bf16[2048,640]{1,0:T(8,128)(2,1)} %bitcast.59), channel_id=1, source_target_pairs={{2,0},{7,1},{4,2},{1,3},{6,4},{3,5},{0,6},{5,7},{10,8},{15,9},{12,... | collective-permute-start | bytes 7864328 | tf_op jit(solution)/shard_map/ppermute | solution.py:341
  15.4 115.6 %collective-permute-start.1 = (bf16[2048,640]{1,0:T(8,128)(2,1)}, bf16[2048,640]{1,0:T(8,128)(2,1)}, u32[]{:S(2)}, u32[]{:S(2)}) collective-permute-start(bf16[2048,640]{1,0:T(8,128)(2,1)} %bitcast.64), channel_id=1, source_target_pairs={{0,1},{1,0},{2,3},{3,2},{4,5},{5,4},{6,7},{7,6},{8,9},{9,8},{10,11... | collective-permute-start | bytes 7864328 | tf_op jit(solution)/shard_map/ppermute | solution.py:340
  15.4 65.4 %collective-permute-start.4 = (bf16[2048,640]{1,0:T(8,128)(2,1)}, bf16[2048,640]{1,0:T(8,128)(2,1)}, u32[]{:S(2)}, u32[]{:S(2)}) collective-permute-start(bf16[2048,640]{1,0:T(8,128)(2,1)} %bitcast.65), channel_id=1, source_target_pairs={{2,0},{7,1},{4,2},{1,3},{6,4},{3,5},{0,6},{5,7},{10,8},{15,9},{12,... | collective-permute-start | bytes 7864328 | tf_op jit(solution)/shard_map/ppermute | solution.py:341
  16.3 85.2 %collective-permute-start.5 = (bf16[640,2048]{1,0:T(8,128)(2,1)}, bf16[640,2048]{1,0:T(8,128)(2,1)}, u32[]{:S(2)}, u32[]{:S(2)}) collective-permute-start(bf16[640,2048]{1,0:T(8,128)(2,1)} %bitcast.70), channel_id=1, source_target_pairs={{2,0},{7,1},{4,2},{1,3},{6,4},{3,5},{0,6},{5,7},{10,8},{15,9},{12,... | collective-permute-start | bytes 7864328 | tf_op jit(solution)/shard_map/ppermute | solution.py:341
  55.0 14.8 %all-to-all-start.1 = ((bf16[16,128,128]{2,1,0:T(8,128)(2,1)}), bf16[16,128,128]{2,1,0:T(8,128)(2,1)S(1)}, u32[]{:S(2)}, u32[]{:S(2)}) async-start(bf16[16,128,128]{2,1,0:T(8,128)(2,1)} %mixer.1), calls=%async_computation.1 | async-start | bytes 1048576 | tf_op jit(solution)/shard_map/all_to_all | solution.py:337
  78.3 55.8 %copy-start.13 = (f32[1,128,2]{1,2,0:T(2,128)S(1)}, f32[1,128,2]{1,2,0:T(2,128)}, u32[]{:S(2)}) copy-start(f32[1,128,2]{1,2,0:T(2,128)} %param.26) | copy-start | bytes 3076
  78.4 55.8 %collective-permute-start.2 = (bf16[640,2048]{1,0:T(8,128)(2,1)S(1)}, bf16[640,2048]{1,0:T(8,128)(2,1)}, u32[]{:S(2)}, u32[]{:S(2)}) collective-permute-start(bf16[640,2048]{1,0:T(8,128)(2,1)S(1)} %bitcast.75), channel_id=1, source_target_pairs={{0,1},{1,0},{2,3},{3,2},{4,5},{5,4},{6,7},{7,6},{8,9},{9,8},{10,11... | collective-permute-start | bytes 7864328 | tf_op jit(solution)/shard_map/ppermute | solution.py:340
  101.5 48.1 %collective-permute-start.6 = (bf16[2048,640]{1,0:T(8,128)(2,1)}, bf16[2048,640]{1,0:T(8,128)(2,1)}, u32[]{:S(2)}, u32[]{:S(2)}) collective-permute-start(bf16[2048,640]{1,0:T(8,128)(2,1)} %collective-permute-done.3.refs_7_), channel_id=1, source_target_pairs={{0,1},{1,0},{2,3},{3,2},{4,5},{5,4},{6,7},{7,6},{8,9},{9,8},{10,11... | collective-permute-start | bytes 7864328 | tf_op jit(solution)/shard_map/ppermute | solution.py:369
  102.4 47.2 %collective-permute-start.7 = (bf16[2048,640]{1,0:T(8,128)(2,1)}, bf16[2048,640]{1,0:T(8,128)(2,1)}, u32[]{:S(2)}, u32[]{:S(2)}) collective-permute-start(bf16[2048,640]{1,0:T(8,128)(2,1)} %collective-permute-done.4.refs_8_), channel_id=1, source_target_pairs={{0,1},{1,0},{2,3},{3,2},{4,5},{5,4},{6,7},{7,6},{8,9},{9,8},{10,11... | collective-permute-start | bytes 7864328 | tf_op jit(solution)/shard_map/ppermute | solution.py:369
  102.4 47.2 %collective-permute-start.8 = (bf16[640,2048]{1,0:T(8,128)(2,1)}, bf16[640,2048]{1,0:T(8,128)(2,1)}, u32[]{:S(2)}, u32[]{:S(2)}) collective-permute-start(bf16[640,2048]{1,0:T(8,128)(2,1)} %collective-permute-done.5.refs_9_), channel_id=1, source_target_pairs={{0,1},{1,0},{2,3},{3,2},{4,5},{5,4},{6,7},{7,6},{8,9},{9,8},{10,11... | collective-permute-start | bytes 7864328 | tf_op jit(solution)/shard_map/ppermute | solution.py:369
  126.6 19.9 %all-to-all-start.4 = ((bf16[16,16,2048]{2,1,0:T(8,128)(2,1)}), bf16[16,16,2048]{2,1,0:T(8,128)(2,1)}, u32[]{:S(2)}, u32[]{:S(2)}) async-start(bf16[16,16,2048]{2,1,0:T(8,128)(2,1)} %bitcast.80), calls=%async_computation.4 | async-start | bytes 2097152 | tf_op jit(solution)/shard_map/all_to_all | solution.py:337
  131.0 34.9 %collective-permute-start.9 = (bf16[16,16,2048]{2,1,0:T(8,128)(2,1)}, bf16[16,16,2048]{2,1,0:T(8,128)(2,1)}, u32[]{:S(2)}, u32[]{:S(2)}) collective-permute-start(bf16[16,16,2048]{2,1,0:T(8,128)(2,1)} %all_to_all.35), channel_id=1, source_target_pairs={{0,4},{1,5},{2,6},{3,7},{4,0},{5,1},{6,2},{7,3},{8,12},{9,13},{10,... | collective-permute-start | bytes 3145736 | tf_op jit(solution)/shard_map/ppermute | solution.py:374
  146.5 50.7 %collective-permute-start.11 = (bf16[16,16,2048]{2,1,0:T(8,128)(2,1)}, bf16[16,16,2048]{2,1,0:T(8,128)(2,1)S(1)}, u32[]{:S(2)}, u32[]{:S(2)}) collective-permute-start(bf16[16,16,2048]{2,1,0:T(8,128)(2,1)} %all-to-all-done.4), channel_id=1, source_target_pairs={{0,4},{1,5},{2,6},{3,7},{4,0},{5,1},{6,2},{7,3},{8,12},{9,13},{10,... | collective-permute-start | bytes 3145736 | tf_op jit(solution)/shard_map/ppermute | solution.py:374
  181.1 35.5 %collective-permute-start.10 = (bf16[16,16,2048]{2,1,0:T(8,128)(2,1)S(1)}, bf16[16,16,2048]{2,1,0:T(8,128)(2,1)S(1)}, u32[]{:S(2)}, u32[]{:S(2)}) collective-permute-start(bf16[16,16,2048]{2,1,0:T(8,128)(2,1)S(1)} %shard_map.146.refs_13_), channel_id=1, source_target_pairs={{0,4},{1,5},{2,6},{3,7},{4,0},{5,1},{6,2},{7,3},{8,12},{9,13},{10,... | collective-permute-start | bytes 3145736 | tf_op jit(solution)/shard_map/ppermute | solution.py:387
  198.2 18.4 %copy-start.1 = (bf16[16,16,2048]{2,1,0:T(8,128)(2,1)S(1)}, bf16[16,16,2048]{2,1,0:T(8,128)(2,1)}, u32[]{:S(2)}) copy-start(bf16[16,16,2048]{2,1,0:T(8,128)(2,1)} %copy-done) | copy-start | bytes 3145732
  213.5 11.9 %collective-permute-start.12 = (bf16[16,8,2048]{2,1,0:T(8,128)(2,1)S(1)}, bf16[16,8,2048]{2,1,0:T(8,128)(2,1)}, u32[]{:S(2)}, u32[]{:S(2)}) collective-permute-start(bf16[16,8,2048]{2,1,0:T(8,128)(2,1)S(1)} %get-tuple-element.24), channel_id=1, source_target_pairs={{0,4},{1,5},{2,6},{3,7},{4,0},{5,1},{6,2},{7,3},{8,12},{9,13},{10,... | collective-permute-start | bytes 1572872 | tf_op jit(solution)/shard_map/ppermute | solution.py:387
  215.7 21.0 %collective-permute-start.13 = (bf16[16,8,2048]{2,1,0:T(8,128)(2,1)S(1)}, bf16[16,8,2048]{2,1,0:T(8,128)(2,1)}, u32[]{:S(2)}, u32[]{:S(2)}) collective-permute-start(bf16[16,8,2048]{2,1,0:T(8,128)(2,1)S(1)} %get-tuple-element.26), channel_id=1, source_target_pairs={{0,4},{1,5},{2,6},{3,7},{4,0},{5,1},{6,2},{7,3},{8,12},{9,13},{10,... | collective-permute-start | bytes 1572872 | tf_op jit(solution)/shard_map/ppermute | solution.py:387
  218.0 20.8 %all-to-all-start.3 = ((bf16[16,16,2048]{2,1,0:T(8,128)(2,1)}), bf16[16,16,2048]{2,1,0:T(8,128)(2,1)S(1)}, u32[]{:S(2)}, u32[]{:S(2)}) async-start(bf16[16,16,2048]{2,1,0:T(8,128)(2,1)} %add_convert_fusion), calls=%async_computation.3 | async-start | bytes 2097152 | tf_op jit(solution)/shard_map/all_to_all | solution.py:337
  222.9 22.3 %copy-start.11 = (bf16[128,512]{0,1:T(8,128)(2,1)S(1)}, bf16[128,512]{0,1:T(8,128)(2,1)}, u32[]{:S(2)}) copy-start(bf16[128,512]{0,1:T(8,128)(2,1)} %get-tuple-element.28) | copy-start | bytes 393220
  238.7 15.9 %all-to-all-start.5 = ((bf16[16,8,2048]{2,1,0:T(8,128)(2,1)}), bf16[16,8,2048]{2,1,0:T(8,128)(2,1)S(1)}, u32[]{:S(2)}, u32[]{:S(2)}) async-start(bf16[16,8,2048]{2,1,0:T(8,128)(2,1)} %add_convert_fusion.2), calls=%async_computation.5 | async-start | bytes 1048576 | tf_op jit(solution)/shard_map/all_to_all | solution.py:337
  254.7 12.5 %all-to-all-start.6 = ((bf16[16,8,2048]{2,1,0:T(8,128)(2,1)}), bf16[16,8,2048]{2,1,0:T(8,128)(2,1)S(1)}, u32[]{:S(2)}, u32[]{:S(2)}) async-start(bf16[16,8,2048]{2,1,0:T(8,128)(2,1)} %add_convert_fusion.1), calls=%async_computation.6 | async-start | bytes 1048576 | tf_op jit(solution)/shard_map/all_to_all | solution.py:337
  (10 other events, 36.5 us)
